TPU v7x, 256 devices: a whole 4x4x8 slice. The times are simulated.
256 devices in a mesh: sp: 64 (over z, x, core), tp: 4 (over y).
Axes of the slice: x: 4, y: 4, z: 8, core: 2. Of those that a mesh axis runs over, the one named last changes fastest.
Arguments:
- full_queries: bfloat16 [8192, 1024], P('sp', 'tp'), may hold values from -7 to 7
- full_keys: bfloat16 [8192, 512], P('sp', 'tp'), may hold values from -6 to 6
- full_values: bfloat16 [8192, 512], P('sp', 'tp'), may hold values from -6 to 6
- full_gates: float32 [8192, 8], P(None, 'tp'), may hold values from -4096 to 0, as said below
- half_queries: bfloat16 [8192, 1024], P('sp', 'tp'), may hold values from -7 to 7
- half_keys: bfloat16 [8192, 512], P('sp', 'tp'), may hold values from -6 to 6
- half_values: bfloat16 [8192, 512], P('sp', 'tp'), may hold values from -6 to 6
- half_gates: float32 [8192, 16], P(None, 'tp'), may hold values from -4096 to 0, as said below
- residual: bfloat16 [8192, 4096], P('sp'), may hold values from -48 to 48
- full_output: bfloat16 [1024, 4096], P('tp'), may hold values from -0.25 to 0.25
- half_output: bfloat16 [1024, 4096], P('tp'), may hold values from -0.25 to 0.25
- norm_gain: float32 [4096], replicated, may hold values from 0.1 to 1.9
- routes: int32 [8192, 4], P('sp'), may hold values from 0 to 63, all different within a row; in each aligned block of 32 rows (0 to 31, 32 to 63, ...) at most 4 rows name the same one
- route_weights: float32 [8192, 4], P('sp'), may hold values from 0.25 to 1.25
- expert_gate: bfloat16 [64, 4096, 512], P('sp', None, 'tp'), may hold values from -0.09375 to 0.09375
- expert_up: bfloat16 [64, 4096, 512], P('sp', None, 'tp'), may hold values from -0.09375 to 0.09375
- expert_down: bfloat16 [64, 512, 4096], P('sp', 'tp'), may hold values from -0.25 to 0.25
- shared_gate: bfloat16 [4096, 512], P(None, 'tp'), may hold values from -0.09375 to 0.09375
- shared_up: bfloat16 [4096, 512], P(None, 'tp'), may hold values from -0.09375 to 0.09375
- shared_down: bfloat16 [512, 4096], P('tp'), may hold values from -0.25 to 0.25
Outputs:
- mixed: bfloat16 [8192, 4096], P(('sp', 'tp'))
Inputs may be any that keep to these rules, and one draw needn't show every extreme that they name: `routes`: in each aligned block of 32 rows no expert is named by more than 4 rows; some expert is named by exactly 4 rows in some block. `full_gates`: each column is a running sum of non-positive terms from the first position on. `half_gates`: each column is a running sum of non-positive terms from the first position on.
All inputs are finite; a program needn't handle non-finite values.
Results may differ from a plain program's by a relative error of at most 0.012.
Values may be sent and summed in bfloat16 or wider, within the bound.
A program may use at most 128 MiB of HBM per device.

v0:
```python
import jax
import jax.numpy as jnp
from jax import lax
from jax.sharding import PartitionSpec as P

D = 4096
WD = 128
ND = 64
TOP = 4


def joined_along(blocks, dim):
    blocks = jnp.moveaxis(blocks, 0, dim)
    dims = blocks.shape
    return blocks.reshape(*dims[:dim], dims[dim] * dims[dim + 1], *dims[dim + 2 :])


def from_everyone(x, axis):
    copies = jnp.broadcast_to(x, (lax.axis_size(axis), *x.shape))
    return lax.all_to_all(copies, axis, split_axis=0, concat_axis=0, tiled=True)


def gather_directly(x, axis, dim):
    return joined_along(from_everyone(x, axis), dim)


def in_one_piece(arrays, axis, dim, along):
    both = jnp.concatenate(arrays, axis=along)
    filled, at, outs = (gather_directly(both, axis, dim), 0, [])
    for a in arrays:
        outs.append(lax.slice_in_dim(filled, at, at + a.shape[along], axis=along))
        at += a.shape[along]
    return tuple(outs)


def side_by_side(arrays, axis, dim, along):
    widths = [a.shape[along] for a in arrays]
    both = jnp.concatenate(arrays, axis=along)
    filled = lax.all_gather(both, axis, axis=dim, tiled=True)
    return tuple(jnp.split(filled, [sum(widths[:k]) for k in range(1, len(widths))], axis=along))


def group_setup(queries, gates, offset, key_heads, head_dim):
    row_count = queries.shape[0]
    group_size = queries.shape[1] // head_dim // key_heads
    shaped = queries.reshape(row_count, key_heads, group_size, head_dim)
    own_gates = lax.dynamic_slice_in_dim(gates, offset, row_count, 0)
    query_gates = jnp.transpose(own_gates.reshape(row_count, key_heads, group_size), (1, 2, 0))[
        ..., None
    ]
    return (shaped, query_gates)


def empty_state(shaped):
    row_count, key_heads, group_size, head_dim = shaped.shape
    return (
        jnp.full((key_heads, group_size, row_count), -1e30, jnp.float32),
        jnp.zeros((key_heads, group_size, row_count), jnp.float32),
        jnp.zeros((key_heads, group_size, row_count, head_dim), jnp.float32),
    )


def group_update(
    running, shaped, query_gates, all_gates, key_rows, value_rows, span_start, query_pos, head_dim
):
    row_max, row_total, weighted = running
    key_count = key_rows.shape[0]
    key_heads = shaped.shape[1]
    group_size = shaped.shape[2]
    key_shaped = key_rows.reshape(key_count, key_heads, head_dim)
    value_shaped = value_rows.reshape(key_count, key_heads, head_dim)
    key_gates = lax.dynamic_slice_in_dim(all_gates, span_start, key_count, 0)
    key_gates = jnp.transpose(key_gates.reshape(key_count, key_heads, group_size), (1, 2, 0))[
        :, :, None, :
    ]
    scores = jnp.einsum("tkgd,skd->kgts", shaped, key_shaped, preferred_element_type=jnp.float32)
    scores = scores * head_dim ** (-0.5) + query_gates - key_gates
    key_pos = span_start + jnp.arange(key_count, dtype=jnp.int32)
    allowed = key_pos[None, :] <= query_pos[:, None]
    masked = jnp.where(allowed, scores, -1e30)
    new_max = jnp.maximum(row_max, jnp.max(masked, axis=-1))
    weights = jnp.where(allowed, jnp.exp(masked - new_max[..., None]), 0.0)
    shrink = jnp.exp(row_max - new_max)
    new_total = row_total * shrink + jnp.sum(weights, axis=-1)
    new_weighted = weighted * shrink[..., None] + jnp.einsum(
        "kgts,skd->kgtd",
        weights.astype(jnp.bfloat16),
        value_shaped,
        preferred_element_type=jnp.float32,
    )
    return (new_max, new_total, new_weighted)


def group_finish(running):
    weighted = running[2] / running[1][..., None]
    row_count = weighted.shape[2]
    return jnp.transpose(weighted, (2, 0, 1, 3)).reshape(row_count, -1).astype(jnp.bfloat16)


def span_for(key_count):
    return max((candidate for candidate in range(1, 2049) if key_count % candidate == 0))


def build_picks(route_rows, experts_count, capacity):
    flat_routes = route_rows.reshape(-1)
    onehot = (flat_routes[:, None] == jnp.arange(experts_count, dtype=jnp.int32)[None, :]).astype(
        jnp.int32
    )
    earlier = jnp.cumsum(onehot, axis=0) - onehot
    slot_rank = jnp.sum(earlier * onehot, axis=1)
    slot_ids = flat_routes * capacity + slot_rank
    picked = slot_ids[:, None] == jnp.arange(experts_count * capacity, dtype=jnp.int32)[None, :]
    return picked.astype(jnp.bfloat16).reshape(
        route_rows.shape[0], route_rows.shape[1], experts_count * capacity
    )


def fill_slots(picked, token_rows):
    occupancy = jnp.sum(picked, axis=1)
    return jnp.einsum(
        "ts,td->sd", occupancy, token_rows, preferred_element_type=jnp.float32
    ).astype(jnp.bfloat16)


def body(
    full_queries,
    full_keys,
    full_values,
    full_gates,
    half_queries,
    half_keys,
    half_values,
    half_gates,
    residual,
    full_output,
    half_output,
    norm_gain,
    routes,
    route_weights,
    expert_gate,
    expert_up,
    expert_down,
    shared_gate,
    shared_up,
    shared_down,
):
    row_count = full_queries.shape[0]
    quarters = lax.axis_size("tp")
    quarter = lax.axis_index("tp")
    quarter_rows = row_count // quarters
    experts_count = lax.axis_size("sp")
    capacity = 2 * quarter_rows * TOP // experts_count
    whole_gate, whole_up, whole_down = (
        *in_one_piece((expert_gate, expert_up), "tp", 2, 0),
        gather_directly(expert_down, "tp", 1),
    )
    offset = lax.axis_index("sp") * row_count
    last_row = offset + row_count - 1
    query_pos = offset + jnp.arange(row_count, dtype=jnp.int32)
    full_shaped, full_query_gates = group_setup(
        full_queries, full_gates, offset, full_keys.shape[1] // WD, WD
    )
    half_shaped, half_query_gates = group_setup(
        half_queries, half_gates, offset, half_keys.shape[1] // ND, ND
    )
    initial = empty_state(full_shaped) + empty_state(half_shaped)
    members = side_by_side((full_keys, full_values, half_keys, half_values), "sp", 0, 1)
    first_key = jnp.int32(0)
    key_count = members[0].shape[0]
    span_rows = span_for(key_count)

    def one_span(running, span_index):
        span_start = first_key + span_index * span_rows
        sliced = tuple(
            (
                lax.dynamic_slice_in_dim(member, span_index * span_rows, span_rows, 0)
                for member in members
            )
        )

        def update(current):
            full_new = group_update(
                current[:3],
                full_shaped,
                full_query_gates,
                full_gates,
                sliced[0],
                sliced[1],
                span_start,
                query_pos,
                WD,
            )
            half_new = group_update(
                current[3:],
                half_shaped,
                half_query_gates,
                half_gates,
                sliced[2],
                sliced[3],
                span_start,
                query_pos,
                ND,
            )
            return full_new + half_new

        return (
            lax.cond(span_start <= last_row, update, lambda unchanged: unchanged, running),
            None,
        )

    result, _ = lax.scan(one_span, initial, jnp.arange(key_count // span_rows, dtype=jnp.int32))
    full_attention = group_finish(result[:3])
    half_attention = group_finish(result[3:])
    partial_out = jnp.dot(
        full_attention, full_output, preferred_element_type=jnp.float32
    ) + jnp.dot(half_attention, half_output, preferred_element_type=jnp.float32)
    middle = residual.astype(jnp.float32) + lax.psum(partial_out.astype(jnp.bfloat16), "tp").astype(
        jnp.float32
    )
    normed = (
        middle * lax.rsqrt(jnp.mean(middle * middle, axis=-1, keepdims=True) + 1e-06) * norm_gain
    ).astype(jnp.bfloat16)
    shared_hidden = (
        jax.nn.silu(jnp.dot(normed, shared_gate, preferred_element_type=jnp.float32))
        * jnp.dot(normed, shared_up, preferred_element_type=jnp.float32)
    ).astype(jnp.bfloat16)
    shared_term = jnp.dot(shared_hidden, shared_down, preferred_element_type=jnp.float32).reshape(
        quarters, quarter_rows, D
    )
    own_routes = lax.dynamic_slice_in_dim(routes, quarter * quarter_rows, quarter_rows, 0)
    own_picks = build_picks(own_routes, experts_count, capacity)
    own_normed = lax.dynamic_slice_in_dim(normed, quarter * quarter_rows, quarter_rows, 0)
    buffer_rows = fill_slots(own_picks, own_normed).reshape(experts_count, capacity, D)
    received = lax.all_to_all(buffer_rows, "sp", split_axis=0, concat_axis=0, tiled=True)
    flat_rows = received.reshape(-1, received.shape[-1])
    gate_part = jnp.dot(flat_rows, whole_gate[0], preferred_element_type=jnp.float32)
    up_part = jnp.dot(flat_rows, whole_up[0], preferred_element_type=jnp.float32)
    hidden = (jax.nn.silu(gate_part) * up_part).astype(jnp.bfloat16)
    block_width = hidden.shape[1] // quarters
    total = jnp.zeros((flat_rows.shape[0], received.shape[-1]), jnp.float32)
    for block_index in range(quarters):
        low_edge = block_index * block_width
        product = jnp.dot(
            hidden[:, low_edge : low_edge + block_width],
            whole_down[0, low_edge : low_edge + block_width],
            preferred_element_type=jnp.float32,
        )
        total = total + lax.optimization_barrier(product.astype(jnp.bfloat16)).astype(jnp.float32)
    finished_rows = total.astype(jnp.bfloat16).reshape(received.shape)
    summed = lax.psum_scatter(
        shared_term.astype(jnp.bfloat16), "tp", scatter_dimension=0, tiled=True
    ).astype(jnp.float32)[0]
    returned = lax.all_to_all(finished_rows, "sp", split_axis=0, concat_axis=0, tiled=True)
    gathered = jnp.einsum(
        "tks,sd->tkd",
        own_picks,
        returned.reshape(experts_count * capacity, D),
        preferred_element_type=jnp.float32,
    )
    own_weights = lax.dynamic_slice_in_dim(route_weights, quarter * quarter_rows, quarter_rows, 0)
    routed = jnp.sum(own_weights[..., None] * gathered, axis=1)
    own_middle = lax.dynamic_slice_in_dim(middle, quarter * quarter_rows, quarter_rows, 0)
    return (own_middle + summed + routed).astype(jnp.bfloat16)


def solution(mesh):
    return jax.shard_map(
        body,
        mesh=mesh,
        in_specs=(
            P("sp", "tp"),
            P("sp", "tp"),
            P("sp", "tp"),
            P(None, "tp"),
            P("sp", "tp"),
            P("sp", "tp"),
            P("sp", "tp"),
            P(None, "tp"),
            P("sp", None),
            P("tp", None),
            P("tp", None),
            P(),
            P("sp", None),
            P("sp", None),
            P("sp", None, "tp"),
            P("sp", None, "tp"),
            P("sp", "tp", None),
            P(None, "tp"),
            P(None, "tp"),
            P("tp", None),
        ),
        out_specs=P(("sp", "tp"), None),
        check_vma=False,
    )
```

profile of v0, /device:TPU:2, one launch (start us, length us, event | category | flops | bytes accessed | tf_op | source)
XLA Modules:
  0.0 441.2 jit_solution(1169314710217238917)
XLA Ops:
  6.5 1.0 copy.82
  7.6 0.9 copy.83
  8.4 0.9 copy.84
  9.3 0.9 copy.85
  10.2 0.7 pad_maximum_fusion.1
  10.9 3.0 pad_maximum_fusion
  13.9 4.1 copy.94
  18.0 5.9 %broadcast_in_dim.98 = bf16[4,2,4096,128]{2,3,1,0:T(8,128)(2,1)} broadcast(bf16[2,4096,128]{1,2,0:T(8,128)(2,1)} %copy.94), dimensions={1,2,3} | broadcast | bytes 10485760 | tf_op jit(solution)/shard_map/broadcast_in_dim | solution.py:19
  23.9 5.8 %all-to-all-start.1 = ((bf16[4,2,4096,128]{2,3,1,0:T(8,128)(2,1)}), bf16[4,2,4096,128]{2,3,1,0:T(8,128)(2,1)}, u32[]{:S(2)}, u32[]{:S(2)}) async-start(bf16[4,2,4096,128]{2,3,1,0:T(8,128)(2,1)} %broadcast_in_dim.98), calls=%async_computation.2 | async-start | bytes 16777216 | tf_op jit(solution)/shard_map/all_to_all | solution.py:20
  30.1 0.7 copy.87
  30.8 1.3 fusion.58
  32.1 1.2 constant_dynamic-slice_fusion.5
  33.3 65.8 %all-gather.2.cloned.1.call-done = bf16[8192,512]{0,1:T(8,128)(2,1)} async-done(((bf16[128,512]{0,1:T(8,128)(2,1)}), bf16[8192,512]{0,1:T(8,128)(2,1)}) %all-gather.2.cloned.1.call-update) | async-done | bytes 8388624 | tf_op jit(solution)/shard_map/all_gather | solution.py:39
  99.1 6.0 %fusion.63 = (bf16[8192,128]{0,1:T(8,128)(2,1)}, bf16[8192,128]{0,1:T(8,128)(2,1)}, bf16[8192,128]{0,1:T(8,128)(2,1)}, bf16[8192,128]{0,1:T(8,128)(2,1)}) fusion(bf16[8192,512]{0,1:T(8,128)(2,1)} %all-gather.2.cloned.1.call-done), kind=kLoop, calls=%fused_computation.108 | loop fusion | bytes 16777216 | tf_op jit(solution)/shard_map/split | solution.py:40
  105.1 4.1 copy.88
  109.2 4.1 copy.90
  113.2 0.5 iota.30
  113.8 22.0 %while.21 = (s32[]{:T(128)}, f32[1,2,128]{2,1,0:T(2,128)S(1)}, f32[1,2,128]{2,1,0:T(2,128)S(1)}, f32[1,2,128,128]{3,2,1,0:T(8,128)S(1)}, f32[2,2,128]{2,1,0:T(2,...) while((s32[]{:T(128)}, f32[1,2,128]{2,1,0:T(2,128)S(1)}, ...), condition=%wide.region_7.8_spmd.clone, body=%wide.region_0.7_spmd.clone.sunk | while | flops 554569600 | bytes 25847364 | solution.py:211
  113.8 1.2 dynamic_slice.103
  115.6 0.6 iota.38
  116.2 12.5 %conditional.3 = ((f32[1,2,128]{2,1,0:T(2,128)S(1)}, f32[1,2,128]{2,1,0:T(2,128)S(1)}, f32[1,2,128,128]{3,2,1,0:T(8,128)S(1)}, f32[2,2,128]{2,1,0:T(2,128)S(1)},...) conditional(s32[]{:T(128)} %convert_element_type.173, (f32[1,2,128]{2,1,0:T(2,128)S(1)}, ...), branch_computations={%region_1.1_spmd, %region_2.6_spmd} | conditional | flops 554569600 | bytes 25846418 | solution.py:207
  116.2 1.6 constant_dynamic-slice_fusion.1
  117.8 0.8 constant_dynamic-slice_fusion
  118.8 0.7 broadcast_add_fusion
  119.8 2.3 fusion.61
  122.1 0.8 fusion.5
  122.9 0.8 fusion.15
  123.7 0.8 dynamic-slice_bitcast_fusion
  124.5 1.8 fusion.60
  126.3 1.9 fusion.18
  128.8 1.2 dynamic_slice.103
  130.5 0.6 iota.38
  131.1 1.2 dynamic_slice.103
  132.9 0.6 iota.38
  133.5 1.2 dynamic_slice.103
  135.3 0.6 iota.38
  136.5 1.1 copy-done.6
  137.6 1.5 fusion.34
  140.3 86.9 %all-reduce.2.cloned.1.call-done = bf16[128,4096]{1,0:T(8,128)(2,1)} async-done(((bf16[128,4096]{1,0:T(8,128)(2,1)}), bf16[128,4096]{1,0:T(8,128)(2,1)}) %all-reduce.2.cloned.1.call-update) | async-done | bytes 1048592 | tf_op jit(solution)/shard_map/psum | solution.py:217
  227.2 3.1 convert_add_fusion
  230.8 2.0 convolution_convert_fusion.4
  232.8 4.1 reshape.188
  236.9 62.0 %all_to_all.20 = bf16[64,4,4096]{2,1,0:T(4,128)(2,1)} all-to-all(bf16[64,4,4096]{2,1,0:T(4,128)(2,1)} %reshape.188), channel_id=1, replica_groups=mesh['sp'=64,'tp'=4] {'sp'}, dimensions={0} | all-to-all | bytes 4194304 | tf_op jit(solution)/shard_map/all_to_all | solution.py:234
  299.0 2.5 broadcast_in_dim.99
  301.4 4.8 %all-to-all-start.2 = ((bf16[4,1,128,4096]{3,2,1,0:T(8,128)(2,1)}), bf16[4,1,128,4096]{3,2,1,0:T(8,128)(2,1)}, u32[]{:S(2)}, u32[]{:S(2)}) async-start(bf16[4,1,128,4096]{3,2,1,0:T(8,128)(2,1)} %broadcast_in_dim.99), calls=%async_computation.3 | async-start | bytes 8388608 | tf_op jit(solution)/shard_map/all_to_all | solution.py:20
  306.3 7.7 %copy.101 = bf16[4,2,4096,128]{2,3,0,1:T(8,128)(2,1)} copy(bf16[4,2,4096,128]{2,3,1,0:T(8,128)(2,1)} %all-to-all-done.1) | data formatting | bytes 16777216 | tf_op jit(solution)/shard_map/all_to_all | solution.py:20
  314.0 6.0 %fusion.62 = (bf16[1,4096,4,128]{1,3,2,0:T(8,128)(2,1)}, bf16[1,4096,4,128]{1,3,2,0:T(8,128)(2,1)}) fusion(bf16[2,4096,4,128]{1,3,2,0:T(8,128)(2,1)} %bitcast.132), kind=kLoop, calls=%fused_computation.107 | loop fusion | bytes 16777216 | tf_op jit(solution)/shard_map/slice | solution.py:31
  320.0 4.0 reshape.189
  324.0 4.3 fusion.66
  328.7 1.3 fusion.36
  330.0 23.9 %all-to-all-done.2 = bf16[4,1,128,4096]{3,2,1,0:T(8,128)(2,1)} async-done(((bf16[4,1,128,4096]{3,2,1,0:T(8,128)(2,1)}), bf16[4,1,128,4096]{3,2,1,0:T(8,128)(2,1)}, u32[]{:S(2)}, u32[]{:S(2)}) %all-to-all-start.2) | async-done | bytes 4194336 | tf_op jit(solution)/shard_map/all_to_all | solution.py:20
  353.9 1.9 convolution_convert_fusion.3
  355.8 1.9 convolution_convert_fusion.2
  357.8 1.9 convolution_convert_fusion.1
  359.7 1.9 convolution_convert_fusion
  361.6 2.8 add_convert_fusion
  364.4 4.1 reshape.190
  368.5 7.0 %all-to-all-start.3 = ((bf16[64,4,4096]{2,1,0:T(4,128)(2,1)}), bf16[64,4,4096]{2,1,0:T(4,128)(2,1)}, u32[]{:S(2)}, u32[]{:S(2)}) async-start(bf16[64,4,4096]{2,1,0:T(4,128)(2,1)} %reshape.190), calls=%async_computation.4 | async-start | bytes 4194304 | tf_op jit(solution)/shard_map/all_to_all | solution.py:253
  375.6 1.6 fusion.65
  377.2 3.3 convolution_convert_fusion.5
  380.7 46.0 %all-to-all-done.3 = bf16[64,4,4096]{2,1,0:T(4,128)(2,1)} async-done(((bf16[64,4,4096]{2,1,0:T(4,128)(2,1)}), bf16[64,4,4096]{2,1,0:T(4,128)(2,1)}, u32[]{:S(2)}, u32[]{:S(2)}) %all-to-all-start.3) | async-done | bytes 2097184 | tf_op jit(solution)/shard_map/all_to_all | solution.py:253
  426.7 4.0 reshape.197
  430.6 2.1 fusion.35
  432.8 1.9 fusion.39
  (73 shorter events, 4.0 us)
Async XLA Ops:
  6.5 129.5 %copy-start = (bf16[256,4096]{1,0:T(8,128)(2,1)S(1)}, bf16[256,4096]{1,0:T(8,128)(2,1)}, u32[]{:S(2)}) copy-start(bf16[256,4096]{1,0:T(8,128)(2,1)} %param.33) | copy-start | bytes 6291460
  6.5 92.6 %all-gather.2.cloned.1.call-start = ((), (), s32[]{:S(2)}) async-start(), calls=%async_computation.5 | async-start | bytes 8519680 | tf_op jit(solution)/shard_map/all_gather | solution.py:39
  23.9 5.9 %copy-start.8 = (bf16[128,256]{1,0:T(8,128)(2,1)S(1)}, bf16[128,256]{1,0:T(8,128)(2,1)}, u32[]{:S(2)}) copy-start(bf16[128,256]{1,0:T(8,128)(2,1)} %param.24) | copy-start | bytes 196612
  23.9 6.1 %copy-start.9 = (bf16[128,256]{1,0:T(8,128)(2,1)S(1)}, bf16[128,256]{1,0:T(8,128)(2,1)}, u32[]{:S(2)}) copy-start(bf16[128,256]{1,0:T(8,128)(2,1)} %param.28) | copy-start | bytes 196612
  23.9 213.0 %all-to-all-start.1 = ((bf16[4,2,4096,128]{2,3,1,0:T(8,128)(2,1)}), bf16[4,2,4096,128]{2,3,1,0:T(8,128)(2,1)}, u32[]{:S(2)}, u32[]{:S(2)}) async-start(bf16[4,2,4096,128]{2,3,1,0:T(8,128)(2,1)} %broadcast_in_dim.98), calls=%async_computation.2 | async-start | bytes 16777216 | tf_op jit(solution)/shard_map/all_to_all | solution.py:20
  29.7 197.5 %all-reduce.2.cloned.1.call-start = ((), (), s32[]{:S(2)}) async-start(), calls=%async_computation.6 | async-start | bytes 2097152 | tf_op jit(solution)/shard_map/psum | solution.py:217
  122.9 1.6 copy-start.13
  136.0 1.6 copy-start.6
  137.6 1.5 copy-start.11
  137.6 89.6 %copy-start.1 = (bf16[128,4096]{1,0:T(8,128)(2,1)S(1)}, bf16[128,4096]{1,0:T(8,128)(2,1)}, u32[]{:S(2)}) copy-start(bf16[128,4096]{1,0:T(8,128)(2,1)} %param.32) | copy-start | bytes 3145732
  140.3 90.0 %copy-start.10 = (f32[4096]{0:T(1024)S(1)}, f32[4096]{0:T(1024)}, u32[]{:S(2)}) copy-start(f32[4096]{0:T(1024)} %param.35) | copy-start | bytes 49156
  227.2 3.1 copy-start.2
  227.2 3.1 copy-start.3
  236.9 62.0 %copy-start.7 = (bf16[1,128,4096]{2,1,0:T(8,128)(2,1)S(1)}, bf16[1,128,4096]{2,1,0:T(8,128)(2,1)}, u32[]{:S(2)}) copy-start(bf16[1,128,4096]{2,1,0:T(8,128)(2,1)} %param.40) | copy-start | bytes 3145732
  301.4 52.5 %all-to-all-start.2 = ((bf16[4,1,128,4096]{3,2,1,0:T(8,128)(2,1)}), bf16[4,1,128,4096]{3,2,1,0:T(8,128)(2,1)}, u32[]{:S(2)}, u32[]{:S(2)}) async-start(bf16[4,1,128,4096]{3,2,1,0:T(8,128)(2,1)} %broadcast_in_dim.99), calls=%async_computation.3 | async-start | bytes 8388608 | tf_op jit(solution)/shard_map/all_to_all | solution.py:20
  324.0 4.3 copy-start.4
  324.0 4.7 %copy-start.5 = (bf16[256,4096]{1,0:T(8,128)(2,1)S(1)}, bf16[256,4096]{1,0:T(8,128)(2,1)}, u32[]{:S(2)}) copy-start(bf16[256,4096]{1,0:T(8,128)(2,1)} %reshape.189) | copy-start | bytes 6291460
  368.5 58.2 %all-to-all-start.3 = ((bf16[64,4,4096]{2,1,0:T(4,128)(2,1)}), bf16[64,4,4096]{2,1,0:T(4,128)(2,1)}, u32[]{:S(2)}, u32[]{:S(2)}) async-start(bf16[64,4,4096]{2,1,0:T(4,128)(2,1)} %reshape.190), calls=%async_computation.4 | async-start | bytes 4194304 | tf_op jit(solution)/shard_map/all_to_all | solution.py:253
  375.5 57.3 %reduce-scatter.2.cloned.1.call-start = ((), (), s32[]{:S(2)}) async-start(), calls=%async_computation.7 | async-start | bytes 1310720 | tf_op jit(solution)/shard_map/reduce_scatter | solution.py:250
  377.2 3.3 copy-start.12
Sparse Core Ops, SparseCore 0:
  11.0 88.0 all-gather.1
  139.3 87.8 all-reduce.1
  380.7 25.5 reduce-scatter.1
where the time goes:
time: 444 us; the launch traced here: 441 us
  waiting for transfers between devices  223 us (50%)
  local copies, waits for them, and re-layouts  76.8 us (17%)
  blocking collectives  62 us (14%)
  matrix products  31.2 us (7%)
  starting transfers between devices  17.8 us (4%)
  other arithmetic  14.8 us (3%)
  between operations  13.5 us (3%)
    psum x1, waiting for transfers between devices, body(): lax.psum(partial_out.astype(jnp.bfloat16), 'tp').astype(jnp.float32)  86.9 us
    all_gather x1, waiting for transfers between devices, side_by_side(): filled = lax.all_gather(both, axis, axis=dim, tiled=True)  65.8 us
    all_to_all x1, blocking collectives, body(): lax.all_to_all(buffer_rows, 'sp', split_axis=0, concat_axis=0, tiled=True)  62 us
    all_to_all x1, waiting for transfers between devices, body(): lax.all_to_all(finished_rows, 'sp', split_axis=0, concat_axis=0, tiled=True)  46 us
    all_to_all x2, waiting for transfers between devices, from_everyone(): return lax.all_to_all(copies, axis, split_axis=0, concat_axis=0, tiled=True)  23.9 us
    unnamed x35, local copies, waits for them, and re-layouts  14.3 us
    all_to_all x2, starting transfers between devices, from_everyone(): return lax.all_to_all(copies, axis, split_axis=0, concat_axis=0, tiled=True)  10.7 us
  transfers between devices with their start and end apart: 6, of which 4 were waited for; matrix products, arithmetic and copies ran while one was open for 22% of the time, Pallas kernels for 0%

commit v1 on v0

v1 whole, which is shorter than its diff:
```python
import functools
import heapq

import jax
import jax.numpy as jnp
from jax import lax
from jax.experimental import pallas as pl
from jax.experimental.pallas import tpu as pltpu
from jax.sharding import PartitionSpec as P

D = 4096
LOG2E = 1.4426950408889634
BF = jnp.bfloat16
F32 = jnp.float32
MESH = pl.DeviceIdType.MESH
NEG = -1e30


def kv_schedule():
    def onward(part, dz, dx, link):
        out = []
        if part == 0:
            if link in ("own", "z+", "z-"):
                if link == "own":
                    out += ["z+", "z-"]
                elif link == "z+" and dz < 4:
                    out.append("z+")
                elif link == "z-" and dz > -3:
                    out.append("z-")
                out += ["x+", "x-"]
            elif link == "x+" and dx == 1 and dz % 2 == 0:
                out.append("x+")
            elif link == "x-" and dx == -1 and dz % 2 == 1:
                out.append("x-")
        else:
            if link in ("own", "x+", "x-"):
                if link == "own":
                    out += ["x+", "x-"]
                elif link == "x+" and dx == 1:
                    out.append("x+")
                out += ["z+", "z-"]
            elif link == "z+" and (dz < 3 or (dz == 3 and dx in (0, 1))):
                out.append("z+")
            elif link == "z-" and dz < 0 and (dz > -3 or dx not in (0, 1)):
                out.append("z-")
        return out

    free = {"z+": 0.0, "z-": 0.0, "x+": 0.0, "x-": 0.0}
    heap, events, count = [], [], 0

    def send(now, part, dz, dx, link):
        nonlocal count
        start = max(now, free[link])
        free[link] = start + 1.4
        step = 1 if link[1] == "+" else -1
        ndz, ndx = (dz + step, dx) if link[0] == "z" else (dz, dx + step)
        if link[0] == "z" and ndz == -4:
            ndz = 4
        if link[0] == "x" and ndx == -2:
            ndx = 2
        heapq.heappush(heap, (free[link] + 1.5, count, part, ndz, ndx, link))
        count += 1

    for part in (1, 0):
        for link in onward(part, 0, 0, "own"):
            send(0.0, part, 0, 0, link)
    seen = set()
    while heap:
        now, _, part, dz, dx, link = heapq.heappop(heap)
        assert (part, dz, dx) not in seen
        seen.add((part, dz, dx))
        links = onward(part, dz, dx, link)
        events.append((part, dz, dx, tuple(links)))
        for out in links:
            send(now, part, dz, dx, out)
    assert len(events) == 62
    own = [(part, 0, 0, tuple(onward(part, 0, 0, "own"))) for part in (1, 0)]
    return own, events


def position():
    s = lax.axis_index("sp")
    y = lax.axis_index("tp")
    z, x, c = s // 8, (s // 2) % 4, s % 2
    return s, y, z, x, c


def sp_of(z, x, c):
    return lax.rem(z + 8, 8) * 8 + lax.rem(x + 4, 4) * 2 + c


def greet(peers):
    barrier = pltpu.get_barrier_semaphore()
    for peer in peers:
        pl.semaphore_signal(barrier, inc=1, device_id=peer, device_id_type=MESH)
    pl.semaphore_wait(barrier, len(peers))


class YGather:
    def __init__(self, src, dst, send_sem, recv_sem):
        s, y, *_ = position()
        self.src, self.dst, self.send, self.recv = src, dst, send_sem, recv_sem
        self.y = y
        self.up = (s, lax.rem(y + 1, 4))
        self.down = (s, lax.rem(y + 3, 4))

    def copy(self, half, src_y, way, hop):
        slot = way * 3 + (half if hop == 0 else 2)
        return pltpu.make_async_remote_copy(
            src_ref=self.src[half] if hop == 0 else self.dst(src_y, half),
            dst_ref=self.dst(src_y, half),
            send_sem=self.send.at[slot],
            recv_sem=self.recv.at[slot],
            device_id=self.up if way == 0 else self.down,
            device_id_type=MESH,
        )

    def start(self):
        self.copy(0, self.y, 0, 0).start()
        self.copy(1, self.y, 1, 0).start()
        self.copy(1, self.y, 0, 0).start()
        self.copy(0, self.y, 1, 0).start()

    def relay(self):
        below, above = lax.rem(self.y + 3, 4), lax.rem(self.y + 1, 4)
        self.copy(0, below, 0, 0).wait_recv()
        self.copy(0, below, 0, 1).start()
        self.copy(1, above, 1, 0).wait_recv()
        self.copy(1, above, 1, 1).start()

    def finish(self):
        below, above, far = lax.rem(self.y + 3, 4), lax.rem(self.y + 1, 4), lax.rem(self.y + 2, 4)
        self.copy(1, below, 0, 0).wait_recv()
        self.copy(0, above, 1, 0).wait_recv()
        self.copy(0, far, 0, 1).wait_recv()
        self.copy(1, far, 1, 1).wait_recv()
        self.sent()

    def sent(self):
        below, above = lax.rem(self.y + 3, 4), lax.rem(self.y + 1, 4)
        for half in (0, 1):
            for way in (0, 1):
                self.copy(half, self.y, way, 0).wait_send()
        self.copy(0, below, 0, 1).wait_send()
        self.copy(1, above, 1, 1).wait_send()


def attend_kernel(
    fq, fk, fv, gf, hq, hk, hv, gh, res, wf, wh, gain, eg, eu,
    mid_out, norm_out, gate_out, up_out,
    kva, kvb, qs, acc, mx, tot, att, part, inbox, resv,
    own_sem, kv_send, kv_recv, w_send, w_recv, rs_send, rs_recv, res_sem,
):
    s, y, z, x, c = position()
    sib = (s + 1 - 2 * c, y)
    to = {
        "z+": (sp_of(z + 1, x, c), y),
        "z-": (sp_of(z - 1, x, c), y),
        "x+": (sp_of(z, x + 1, c), y),
        "x-": (sp_of(z, x - 1, c), y),
    }
    others = [(s, lax.rem(y + k, 4)) for k in (2, 1, 3)]
    greet(list(to.values()) + [sib] + others)

    kv = (kva, kvb)
    pieces = [
        (fk, kva, 0), (fv, kva, 128), (hk, kvb, 0), (hv, kvb, 128),
    ]
    own = [
        pltpu.make_async_copy(src, dst.at[s, :, pl.ds(at, 128)], own_sem.at[i])
        for i, (src, dst, at) in enumerate(pieces)
    ]
    for copy in own:
        copy.start()
    res_copy = pltpu.make_async_copy(res.at[pl.ds(y * 32, 32)], resv, res_sem)
    res_copy.start()

    def hop(prt, idx, device):
        return pltpu.make_async_remote_copy(
            src_ref=kv[prt].at[idx],
            dst_ref=kv[prt].at[idx],
            send_sem=kv_send.at[prt],
            recv_sem=kv_recv.at[prt, idx],
            device_id=device,
            device_id_type=MESH,
        )

    own_events, events = kv_schedule()
    for prt, _, _, links in own_events:
        own[2 * prt].wait()
        own[2 * prt + 1].wait()
        for link in links:
            hop(prt, s, to[link]).start()
        hop(prt, s, sib).start()

    half_rows = 2048
    gates = YGather(
        [eg.at[pl.ds(h * half_rows, half_rows)] for h in (0, 1)],
        lambda j, h: gate_out.at[j, pl.ds(h * half_rows, half_rows)],
        w_send.at[0], w_recv.at[0],
    )
    ups = YGather(
        [eu.at[pl.ds(h * 1024, 1024)] for h in (0, 1)],
        lambda j, h: up_out.at[j, pl.ds(h * 1024, 1024)],
        w_send.at[1], w_recv.at[1],
    )
    gates.start()
    ups.start()

    lane = lax.broadcasted_iota(jnp.int32, (128, 128), 1)
    qs[0, 0:128] = fq[:, 0:128]
    qs[0, 128:256] = fq[:, 128:256]
    h01 = hq[:, 0:128].astype(F32)
    h23 = hq[:, 128:256].astype(F32)
    qs[1, 0:128] = jnp.where(lane < 64, h01, 0.0).astype(BF)
    qs[1, 128:256] = jnp.where(lane < 64, pltpu.roll(h01, 64, 1), 0.0).astype(BF)
    qs[2, 0:128] = jnp.where(lane >= 64, pltpu.roll(h23, 64, 1), 0.0).astype(BF)
    qs[2, 128:256] = jnp.where(lane >= 64, h23, 0.0).astype(BF)
    acc[...] = jnp.zeros_like(acc)
    tot[...] = jnp.zeros_like(tot)
    mx[...] = jnp.full_like(mx, NEG)

    for i, (prt, dz, dx, links) in enumerate(events):
        idx = sp_of(z - dz, x - dx, c)
        hop(prt, idx, sib).wait_recv()
        for link in links:
            hop(prt, idx, to[link]).start()
        hop(prt, idx, sib).start()
        if i == 30:
            gates.relay()
    ups.relay()

    @pl.loop(0, 32)
    def _(i):
        idx = 2 * i + 1 - c
        for prt in (0, 1):
            hop(prt, idx, sib).wait_recv()

    row0 = s * 128
    gfirst = gf[:, pl.ds(pl.multiple_of(row0, 128), 128)][:, 0:1]
    hfirst = gh[:, pl.ds(pl.multiple_of(row0, 128), 128)][:, 0:1]

    def chunk(at, masked):
        key0 = pl.multiple_of(at * 1024, 1024)
        fg = (gf[:, pl.ds(key0, 1024)] - gfirst) * LOG2E
        hg = (gh[:, pl.ds(key0, 1024)] - hfirst) * LOG2E
        if masked:
            qpos = (s % 8) * 128 + lax.broadcasted_iota(jnp.int32, (128, 1024), 0)
            kpos = lax.broadcasted_iota(jnp.int32, (128, 1024), 1)
            allowed = kpos <= qpos
        for g in range(3):
            store = kva if g == 0 else kvb
            k = store[pl.ds(at * 8, 8), :, 0:128].reshape(1024, 128)
            v = store[pl.ds(at * 8, 8), :, 128:256].reshape(1024, 128)
            scale = (128 ** -0.5 if g == 0 else 0.125) * LOG2E
            scores = lax.dot_general(
                qs[g], k, (((1,), (1,)), ((), ())), preferred_element_type=F32
            )
            for r in (0, 1):
                row = fg[r : r + 1] if g == 0 else hg[2 * (g - 1) + r : 2 * (g - 1) + r + 1]
                t = scores[r * 128 : (r + 1) * 128] * scale - row
                if masked:
                    t = jnp.where(allowed, t, NEG)
                old = mx[g, pl.ds(r * 128, 128)]
                new = jnp.maximum(old, jnp.max(t, axis=1, keepdims=True))
                p = jnp.exp2(t - new[:, 0:1])
                shrink = jnp.exp2(old - new)
                mx[g, pl.ds(r * 128, 128)] = new
                tot[g, pl.ds(r * 128, 128)] = (
                    tot[g, pl.ds(r * 128, 128)] * shrink + jnp.sum(p, axis=1, keepdims=True)
                )
                acc[g, pl.ds(r * 128, 128)] = acc[g, pl.ds(r * 128, 128)] * shrink + jnp.dot(
                    p.astype(BF), v, preferred_element_type=F32
                )

    @pl.loop(0, z)
    def _(at):
        chunk(at, False)

    chunk(z, True)

    outs = [
        [acc[g, r * 128 : (r + 1) * 128] / tot[g, r * 128 : (r + 1) * 128] for r in (0, 1)]
        for g in range(3)
    ]
    att[:, 0:128] = outs[0][0].astype(BF)
    att[:, 128:256] = outs[0][1].astype(BF)
    att[:, 256:384] = jnp.where(lane < 64, outs[1][0], pltpu.roll(outs[1][1], 64, 1)).astype(BF)
    att[:, 384:512] = jnp.where(lane < 64, pltpu.roll(outs[2][0], 64, 1), outs[2][1]).astype(BF)

    gates.finish()
    ups.finish()

    def share(k, n, device):
        return pltpu.make_async_remote_copy(
            src_ref=part.at[lax.rem(y + k, 4), :, pl.ds(n * 1024, 1024)],
            dst_ref=inbox.at[k - 1, :, pl.ds(n * 1024, 1024)],
            send_sem=rs_send.at[k - 1, n],
            recv_sem=rs_recv.at[k - 1, n],
            device_id=device,
            device_id_type=MESH,
        )

    for n in range(4):
        cols = slice(n * 1024, (n + 1) * 1024)
        product = jnp.dot(att[:, 0:256], wf[:, cols], preferred_element_type=F32) + jnp.dot(
            att[:, 256:512], wh[:, cols], preferred_element_type=F32
        )
        part[:, :, cols] = product.astype(BF).reshape(4, 32, 1024)
        for k, device in zip((2, 1, 3), others):
            share(k, n, device).start()
    res_copy.wait()
    square = jnp.zeros((32, 1), F32)
    for n in range(4):
        cols = slice(n * 1024, (n + 1) * 1024)
        total = resv[:, cols].astype(F32) + part[y, :, cols].astype(F32)
        for k, device in zip((2, 1, 3), others):
            share(k, n, device).wait_recv()
            total = total + inbox[k - 1, :, cols].astype(F32)
        mid_out[:, cols] = total
        square = square + jnp.sum(total * total, axis=1, keepdims=True)
    factor = lax.rsqrt(square * (1.0 / D) + 1e-06)
    norm_out[...] = (mid_out[...] * factor * gain[...]).astype(BF)

    for n in range(4):
        for k, device in zip((2, 1, 3), others):
            share(k, n, device).wait_send()
    for prt in (0, 1):
        everything = kv[prt].at[pl.ds(0, 63)]
        pltpu.make_async_copy(everything, everything, kv_send.at[prt]).wait()


def attend(fq, fk, fv, gf, hq, hk, hv, gh, res, wf, wh, gain, eg, eu):
    vmem = pl.BlockSpec(memory_space=pltpu.VMEM)
    anym = pl.BlockSpec(memory_space=pl.ANY)
    return pl.pallas_call(
        attend_kernel,
        name="attend",
        out_shape=(
            jax.ShapeDtypeStruct((32, D), F32),
            jax.ShapeDtypeStruct((32, D), BF),
            jax.ShapeDtypeStruct((4, 4096, 128), BF),
            jax.ShapeDtypeStruct((4, 2048, 128), BF),
        ),
        in_specs=[vmem, anym, anym, vmem, vmem, anym, anym, vmem, anym, vmem, vmem, vmem, anym, anym],
        out_specs=[vmem, vmem, anym, anym],
        scratch_shapes=[
            pltpu.VMEM((64, 128, 256), BF),
            pltpu.VMEM((64, 128, 256), BF),
            pltpu.VMEM((3, 256, 128), BF),
            pltpu.VMEM((3, 256, 128), F32),
            pltpu.VMEM((3, 256, 128), F32),
            pltpu.VMEM((3, 256, 128), F32),
            pltpu.VMEM((128, 512), BF),
            pltpu.VMEM((4, 32, D), BF),
            pltpu.VMEM((3, 32, D), BF),
            pltpu.VMEM((32, D), BF),
            pltpu.SemaphoreType.DMA((4,)),
            pltpu.SemaphoreType.DMA((2,)),
            pltpu.SemaphoreType.DMA((2, 64)),
            pltpu.SemaphoreType.DMA((2, 6)),
            pltpu.SemaphoreType.DMA((2, 6)),
            pltpu.SemaphoreType.DMA((3, 4)),
            pltpu.SemaphoreType.DMA((3, 4)),
            pltpu.SemaphoreType.DMA,
        ],
        compiler_params=pltpu.CompilerParams(
            collective_id=0, has_side_effects=True, vmem_limit_bytes=56 * 1024 * 1024
        ),
    )(fq, fk, fv, gf, hq, hk, hv, gh, res, wf, wh, gain, eg, eu)


def build_picks(route_rows, experts_count, capacity):
    flat_routes = route_rows.reshape(-1)
    onehot = (flat_routes[:, None] == jnp.arange(experts_count, dtype=jnp.int32)[None, :]).astype(
        jnp.int32
    )
    earlier = jnp.cumsum(onehot, axis=0) - onehot
    slot_rank = jnp.sum(earlier * onehot, axis=1)
    slot_ids = flat_routes * capacity + slot_rank
    picked = slot_ids[:, None] == jnp.arange(experts_count * capacity, dtype=jnp.int32)[None, :]
    return picked.astype(jnp.bfloat16).reshape(
        route_rows.shape[0], route_rows.shape[1], experts_count * capacity
    )


def body(
    full_queries, full_keys, full_values, full_gates, half_queries, half_keys, half_values,
    half_gates, residual, full_output, half_output, norm_gain, routes, route_weights,
    expert_gate, expert_up, expert_down, shared_gate, shared_up, shared_down,
):
    quarter = lax.axis_index("tp")
    middle, normed_own, gates_g, ups_g = attend(
        full_queries, full_keys, full_values, full_gates.T, half_queries, half_keys, half_values,
        half_gates.T, residual, full_output, half_output, norm_gain.reshape(1, D),
        expert_gate[0], expert_up[0],
    )
    own_g = lax.dynamic_update_slice(gates_g, expert_gate, (quarter, 0, 0))
    own_u = lax.dynamic_update_slice(ups_g, expert_up[:, :2048], (quarter, 0, 0))
    whole_gate = jnp.moveaxis(own_g, 0, 1).reshape(4096, 512)
    up_top = jnp.moveaxis(own_u, 0, 1).reshape(2048, 512)
    up_bot = lax.all_gather(expert_up[0, 2048:], "tp", axis=1, tiled=True)
    whole_up = jnp.concatenate([up_top, up_bot], 0)
    whole_down = lax.all_gather(expert_down[0], "tp", axis=0, tiled=True)
    normed = lax.all_gather(normed_own, "tp", axis=0, tiled=True)
    shared_hidden = (
        jax.nn.silu(jnp.dot(normed, shared_gate, preferred_element_type=F32))
        * jnp.dot(normed, shared_up, preferred_element_type=F32)
    ).astype(BF)
    shared_term = jnp.dot(shared_hidden, shared_down, preferred_element_type=F32).reshape(4, 32, D)
    own_routes = lax.dynamic_slice_in_dim(routes, quarter * 32, 32, 0)
    own_picks = build_picks(own_routes, 64, 4)
    occupancy = jnp.sum(own_picks, axis=1)
    buffer_rows = jnp.einsum("ts,td->sd", occupancy, normed_own, preferred_element_type=F32).astype(BF)
    received = lax.all_to_all(buffer_rows.reshape(64, 4, D), "sp", split_axis=0, concat_axis=0, tiled=True)
    flat_rows = received.reshape(-1, D)
    gate_part = jnp.dot(flat_rows, whole_gate, preferred_element_type=F32)
    up_part = jnp.dot(flat_rows, whole_up, preferred_element_type=F32)
    hidden = (jax.nn.silu(gate_part) * up_part).astype(BF)
    finished = jnp.dot(hidden, whole_down, preferred_element_type=F32).astype(BF).reshape(64, 4, D)
    summed = lax.psum_scatter(shared_term.astype(BF), "tp", scatter_dimension=0, tiled=True).astype(F32)[0]
    returned = lax.all_to_all(finished, "sp", split_axis=0, concat_axis=0, tiled=True)
    gathered = jnp.einsum("tks,sd->tkd", own_picks, returned.reshape(256, D), preferred_element_type=F32)
    own_weights = lax.dynamic_slice_in_dim(route_weights, quarter * 32, 32, 0)
    routed = jnp.sum(own_weights[..., None] * gathered, axis=1)
    return (middle + summed + routed).astype(BF)


def solution(mesh):
    return jax.shard_map(
        body,
        mesh=mesh,
        in_specs=(
            P("sp", "tp"), P("sp", "tp"), P("sp", "tp"), P(None, "tp"),
            P("sp", "tp"), P("sp", "tp"), P("sp", "tp"), P(None, "tp"),
            P("sp", None), P("tp", None), P("tp", None), P(), P("sp", None), P("sp", None),
            P("sp", None, "tp"), P("sp", None, "tp"), P("sp", "tp", None),
            P(None, "tp"), P(None, "tp"), P("tp", None),
        ),
        out_specs=P(("sp", "tp"), None),
        check_vma=False,
    )
```

time: 444 us -> 264 us (0.59)
  waiting for transfers between devices: 223 us -> 104 us
  Pallas kernels: 0 us -> 78.3 us
  blocking collectives: 62 us -> 0 us
  local copies, waits for them, and re-layouts: 76.8 us -> 26 us
  other arithmetic: 14.8 us -> 2.64 us
  matrix products: 31.2 us -> 19.3 us
    psum x1 -> x0, waiting for transfers between devices: 86.9 us -> none  [body(): lax.psum(partial_out.astype(jnp.bfloat16), 'tp').astype(jnp.float32)]
    pallas_call x0 -> x1, Pallas kernels: none -> 78.3 us  [attend(): pl.pallas_call(attend_kernel, name='attend', out_shape=(jax.ShapeDtypeStr...]
    all_to_all x1 -> x0, blocking collectives: 62 us -> none  [body(): lax.all_to_all(buffer_rows, 'sp', split_axis=0, concat_axis=0, tiled=True)]
    all_gather x1 -> x3, waiting for transfers between devices: 65.8 us -> 41.4 us  [the longest x1 28.7 us: body(): normed = lax.all_gather(normed_own, 'tp', axis=0, tiled=True)]
    all_to_all x3 -> x2, waiting for transfers between devices: 70 us -> 55.4 us  [the longest x1 38.6 us: body(): lax.all_to_all(buffer_rows.reshape(64, 4, D), 'sp', split_axis=0, concat_...]
    unnamed x35 -> x17, local copies, waits for them, and re-layouts: 14.3 us -> 1.06 us
    dot_general x16 -> x6, matrix products: 31.2 us -> 19.3 us  [the longest x1 7.43 us: body(): jnp.dot(hidden, whole_down, preferred_element_type=F32).astype(BF)]
    transpose x0 -> x2, local copies, waits for them, and re-layouts: none -> 10.4 us  [the longest x1 6.41 us: body(): whole_gate = jnp.moveaxis(own_g, 0, 1).reshape(4096, 512)]
  transfers between devices with their start and end apart: 6 -> 6, of which waited for: 4 -> 5; matrix products, arithmetic and copies ran while one was open for 22% -> 12% of each run, Pallas kernels for 0% -> 0%
where the time goes in v1:
time: 264 us; the launch traced here: 263 us
  waiting for transfers between devices  104 us (39%)
  Pallas kernels  78.3 us (30%)
  local copies, waits for them, and re-layouts  26 us (10%)
  starting transfers between devices  19.3 us (7%)
  matrix products  19.3 us (7%)
  between operations  13.3 us (5%)
  other arithmetic  2.64 us (1%)
    pallas_call x1, Pallas kernels, attend(): pl.pallas_call(attend_kernel, name='attend', out_shape=(jax.ShapeDtypeStr...  78.3 us
    all_to_all x1, waiting for transfers between devices, body(): lax.all_to_all(buffer_rows.reshape(64, 4, D), 'sp', split_axis=0, concat_...  38.6 us
    all_gather x1, waiting for transfers between devices, body(): normed = lax.all_gather(normed_own, 'tp', axis=0, tiled=True)  28.7 us
    all_to_all x1, waiting for transfers between devices, body(): lax.all_to_all(finished, 'sp', split_axis=0, concat_axis=0, tiled=True)  16.8 us
    all_gather x1, waiting for transfers between devices, body(): whole_down = lax.all_gather(expert_down[0], 'tp', axis=0, tiled=True)  12.7 us
    all_to_all x1, starting transfers between devices, body(): lax.all_to_all(finished, 'sp', split_axis=0, concat_axis=0, tiled=True)  10.8 us
    all_to_all x1, starting transfers between devices, body(): lax.all_to_all(buffer_rows.reshape(64, 4, D), 'sp', split_axis=0, concat_...  8.32 us
    dot_general x1, matrix products, body(): jnp.dot(hidden, whole_down, preferred_element_type=F32).astype(BF)  7.43 us
  transfers between devices with their start and end apart: 6, of which 5 were waited for; matrix products, arithmetic and copies ran while one was open for 12% of the time, Pallas kernels for 0%

profile of v1, /device:TPU:2, one launch (start us, length us, event | category | flops | bytes accessed | tf_op | source)
XLA Modules:
  0.0 263.1 jit_solution(2316059966114211864)
XLA Ops:
  6.5 0.0 copy-start
  6.5 0.0 all-gather.8.cloned.1.call-start
  6.5 0.0 copy-start.2
  6.5 78.3 %attend.1 = (f32[32,4096]{1,0:T(8,128)}, bf16[32,4096]{1,0:T(8,128)(2,1)}, bf16[4,4096,128]{2,1,0:T(8,128)(2,1)}, bf16[4,2048,128]{2,1,0:T(8,128)(2,1)}) custom-call(bf16[128,256]{1,0:T(8,128)(2,1)} %fq.1, bf16[128,128]{1,0:T(8,128)(2,1)} %fk.1, bf16[128,128]{1,0:T(8,128)(2,1)} %fv.1, f32[2,8192]{1,0:T(2,128)} %bitcast.39, bf16[128,256]{1,0:T(8,128)(2,1)} %hq.1, ...), custom_call_target="tpu_custom_call" | custom-call | tf_op jit(solution)/shard_map/attend/pallas_call | solution.py:336
  84.9 0.0 copy-done.2
  84.9 0.0 copy-start.6
  84.9 0.0 copy-start.4
  84.9 0.9 slice_dynamic-update-slice_fusion
  85.8 1.0 copy.39
  86.8 0.0 all-gather.8.cloned.1.call-update
  86.8 0.0 all-gather.10.cloned.1.call-start
  86.9 0.7 all-gather.10.cloned.1.call-update
  87.6 0.0 copy-done.6
  87.6 0.1 constant_dynamic-slice_fusion
  87.7 0.1 copy.34
  87.8 0.1 eq.51
  87.9 0.1 fusion.22
  88.0 0.2 reduce_window_sum.11
  88.1 0.2 select_reduce_fusion
  88.3 0.1 reduce_sum.33
  88.4 0.1 copy.35
  88.5 0.1 multiply_add_fusion
  88.6 0.1 fusion.20
  88.7 0.0 copy-done.4
  88.7 0.7 convolution_convert_fusion.1
  89.4 2.2 reshape.66
  91.6 8.3 %all-to-all-start = ((bf16[64,4,4096]{2,1,0:T(4,128)(2,1)}), bf16[64,4,4096]{2,1,0:T(4,128)(2,1)S(1)}, u32[]{:S(2)}, u32[]{:S(2)}) async-start(bf16[64,4,4096]{2,1,0:T(4,128)(2,1)} %reshape.66), calls=%async_computation.1 | async-start | bytes 4194304 | tf_op jit(solution)/shard_map/all_to_all | solution.py:415
  100.0 2.3 constant_dynamic-update-slice_fusion
  102.2 6.4 %copy.36 = bf16[4096,4,128]{0,2,1:T(8,128)(2,1)} copy(bf16[4096,4,128]{2,0,1:T(8,128)(2,1)} %bitcast.31) | data formatting | bytes 8388608 | tf_op jit(solution)/shard_map/transpose | solution.py:400
  108.6 4.0 %copy.37 = bf16[2048,4,128]{0,2,1:T(8,128)(2,1)} copy(bf16[2048,4,128]{2,0,1:T(8,128)(2,1)} %bitcast.37) | data formatting | bytes 4194304 | tf_op jit(solution)/shard_map/transpose | solution.py:401
  112.6 38.6 %all-to-all-done = bf16[64,4,4096]{2,1,0:T(4,128)(2,1)S(1)} async-done(((bf16[64,4,4096]{2,1,0:T(4,128)(2,1)}), bf16[64,4,4096]{2,1,0:T(4,128)(2,1)S(1)}, u32[]{:S(2)}, u32[]{:S(2)}) %all-to-all-start) | async-done | bytes 2097184 | tf_op jit(solution)/shard_map/all_to_all | solution.py:415
  151.2 2.0 reshape.67
  153.2 0.0 copy-start.3
  153.2 5.1 %fusion.34 = f32[256,512]{1,0:T(8,128)} fusion(bf16[256,4096]{1,0:T(8,128)(2,1)} %reshape.67, bf16[4096,512]{0,1:T(8,128)(2,1)} %bitcast.32), kind=kOutput, calls=%fused_computation.41 | convolution fusion | flops 1073741824 | bytes 6815744 | tf_op jit(solution)/shard_map/dot_general | solution.py:417
  158.3 0.0 all-gather.8.cloned.1.call-done
  158.3 12.7 %all-gather.10.cloned.1.call-done = bf16[1,512,4096]{2,1,0:T(8,128)(2,1)} async-done(((bf16[1,128,4096]{2,1,0:T(8,128)(2,1)}), bf16[1,512,4096]{2,1,0:T(8,128)(2,1)}) %all-gather.10.cloned.1.call-update) | async-done | bytes 4194320 | tf_op jit(solution)/shard_map/all_gather | solution.py:404
  171.0 0.0 copy-done.3
  171.1 7.4 %convolution_convert_fusion = bf16[256,4096]{1,0:T(8,128)(2,1)} fusion(bf16[1,512,4096]{2,1,0:T(8,128)(2,1)} %all-gather.10.cloned.1.call-done, bf16[256,4096]{1,0:T(8,128)(2,1)} %reshape.67, bf16[2048,512]{0,1:T(8,128)(2,1)} %bitcast.41, bf16[2048,512]{0,1:T(8,128)(2,1)S(1)} %bitcast.36, f32[256,512]{1,0:T(8,128)} %fusion.34), kind=kOutput, calls=%fused_computation | convolution fusion | flops 2157707264 | bytes 13107200 | tf_op jit(solution)/shard_map/dot_general | solution.py:420
  178.5 4.1 %reshape.70 = bf16[64,4,4096]{2,1,0:T(4,128)(2,1)} reshape(bf16[256,4096]{1,0:T(8,128)(2,1)} %convolution_convert_fusion) | data formatting | bytes 4194304 | tf_op jit(solution)/shard_map/reshape | solution.py:420
  182.6 0.0 copy-start.5
  182.6 10.8 %all-to-all-start.1 = ((bf16[64,4,4096]{2,1,0:T(4,128)(2,1)}), bf16[64,4,4096]{2,1,0:T(4,128)(2,1)}, u32[]{:S(2)}, u32[]{:S(2)}) async-start(bf16[64,4,4096]{2,1,0:T(4,128)(2,1)} %reshape.70), calls=%async_computation.2 | async-start | bytes 4194304 | tf_op jit(solution)/shard_map/all_to_all | solution.py:422
  193.4 0.0 all-gather.6.cloned.1.call-start
  193.5 0.7 all-gather.6.cloned.1.call-update
  194.2 0.0 reduce-scatter.2.cloned.1.call-start
  194.2 28.7 %all-gather.6.cloned.1.call-done = bf16[128,4096]{1,0:T(8,128)(2,1)} async-done(((bf16[32,4096]{1,0:T(8,128)(2,1)}), bf16[128,4096]{1,0:T(8,128)(2,1)}) %all-gather.6.cloned.1.call-update) | async-done | bytes 1048592 | tf_op jit(solution)/shard_map/all_gather | solution.py:405
  222.9 0.0 copy-done.5
  222.9 0.0 copy-start.1
  222.9 1.7 fusion.33
  224.6 0.0 copy-done
  224.6 0.0 copy-done.1
  224.6 0.0 copy-start.7
  224.6 3.0 %convolution_convert_fusion.2 = bf16[128,4096]{1,0:T(8,128)(2,1)} fusion(bf16[128,4096]{1,0:T(8,128)(2,1)S(1)} %copy-done, bf16[128,4096]{1,0:T(8,128)(2,1)S(1)} %copy-done.1, bf16[4096,128]{1,0:T(8,128)(2,1)} %param.38, f32[128,128]{1,0:T(8,128)S(1)} %fusion.33), kind=kOutput, calls=%fused_computation.3 | convolution fusion | flops 269058048 | bytes 4259840 | tf_op jit(solution)/shard_map/dot_general | solution.py:410
  227.7 0.0 reduce-scatter.2.cloned.1.call-update
  227.7 0.0 copy-done.7
  227.7 0.1 constant_dynamic-slice_fusion.1
  227.8 16.8 %all-to-all-done.1 = bf16[64,4,4096]{2,1,0:T(4,128)(2,1)} async-done(((bf16[64,4,4096]{2,1,0:T(4,128)(2,1)}), bf16[64,4,4096]{2,1,0:T(4,128)(2,1)}, u32[]{:S(2)}, u32[]{:S(2)}) %all-to-all-start.1) | async-done | bytes 2097184 | tf_op jit(solution)/shard_map/all_to_all | solution.py:422
  244.6 2.6 reshape.75
  247.2 1.3 fusion.5
  248.5 6.1 %reduce-scatter.2.cloned.1.call-done = bf16[1,32,4096]{2,1,0:T(8,128)(2,1)} async-done(((bf16[4,32,4096]{2,1,0:T(8,128)(2,1)}), bf16[1,32,4096]{2,1,0:T(8,128)(2,1)}) %reduce-scatter.2.cloned.1.call-update) | async-done | bytes 262160 | tf_op jit(solution)/shard_map/reduce_scatter | solution.py:421
  254.5 2.0 fusion.14
Async XLA Ops:
  6.5 218.1 %copy-start = (bf16[128,4096]{1,0:T(8,128)(2,1)S(1)}, bf16[128,4096]{1,0:T(8,128)(2,1)}, u32[]{:S(2)}) copy-start(bf16[128,4096]{1,0:T(8,128)(2,1)} %param.39) | copy-start | bytes 3145732
  6.5 151.8 %all-gather.8.cloned.1.call-start = ((), (), s32[]{:S(2)}) async-start(), calls=%async_computation.5 | async-start | bytes 2621440 | tf_op jit(solution)/shard_map/all_gather | solution.py:402
  6.5 78.3 %copy-start.2 = (bf16[1,4096,128]{2,1,0:T(8,128)(2,1)S(1)}, bf16[1,4096,128]{2,1,0:T(8,128)(2,1)}, u32[]{:S(2)}) copy-start(bf16[1,4096,128]{2,1,0:T(8,128)(2,1)} %param.35) | copy-start | bytes 3145732
  84.9 2.7 %copy-start.6 = (s32[128,4]{0,1:T(4,128)S(1)}, s32[128,4]{0,1:T(4,128)}, u32[]{:S(2)}) copy-start(s32[128,4]{0,1:T(4,128)} %param.32) | copy-start | bytes 6148
  84.9 3.8 %copy-start.4 = (bf16[32,4096]{1,0:T(8,128)(2,1)S(1)}, bf16[32,4096]{1,0:T(8,128)(2,1)}, u32[]{:S(2)}) copy-start(bf16[32,4096]{1,0:T(8,128)(2,1)} %get-tuple-element.10) | copy-start | bytes 786436
  86.8 84.2 %all-gather.10.cloned.1.call-start = ((), (), s32[]{:S(2)}) async-start(), calls=%async_computation.6 | async-start | bytes 5242880 | tf_op jit(solution)/shard_map/all_gather | solution.py:404
  91.6 59.6 %all-to-all-start = ((bf16[64,4,4096]{2,1,0:T(4,128)(2,1)}), bf16[64,4,4096]{2,1,0:T(4,128)(2,1)S(1)}, u32[]{:S(2)}, u32[]{:S(2)}) async-start(bf16[64,4,4096]{2,1,0:T(4,128)(2,1)} %reshape.66), calls=%async_computation.1 | async-start | bytes 4194304 | tf_op jit(solution)/shard_map/all_to_all | solution.py:415
  153.2 17.8 %copy-start.3 = (bf16[2048,4,128]{0,2,1:T(8,128)(2,1)S(1)}, bf16[2048,4,128]{0,2,1:T(8,128)(2,1)}, u32[]{:S(2)}) copy-start(bf16[2048,4,128]{0,2,1:T(8,128)(2,1)} %copy.37) | copy-start | bytes 6291460
  182.6 40.3 %copy-start.5 = (bf16[4096,128]{1,0:T(8,128)(2,1)S(1)}, bf16[4096,128]{1,0:T(8,128)(2,1)}, u32[]{:S(2)}) copy-start(bf16[4096,128]{1,0:T(8,128)(2,1)} %param.37) | copy-start | bytes 3145732
  182.6 62.0 %all-to-all-start.1 = ((bf16[64,4,4096]{2,1,0:T(4,128)(2,1)}), bf16[64,4,4096]{2,1,0:T(4,128)(2,1)}, u32[]{:S(2)}, u32[]{:S(2)}) async-start(bf16[64,4,4096]{2,1,0:T(4,128)(2,1)} %reshape.70), calls=%async_computation.2 | async-start | bytes 4194304 | tf_op jit(solution)/shard_map/all_to_all | solution.py:422
  193.4 29.4 %all-gather.6.cloned.1.call-start = ((), (), s32[]{:S(2)}) async-start(), calls=%async_computation.3 | async-start | bytes 1310720 | tf_op jit(solution)/shard_map/all_gather | solution.py:405
  194.2 60.4 %reduce-scatter.2.cloned.1.call-start = ((), (), s32[]{:S(2)}) async-start(), calls=%async_computation.4 | async-start | bytes 1310720 | tf_op jit(solution)/shard_map/reduce_scatter | solution.py:421
  222.9 1.8 copy-start.1
  224.6 3.0 %copy-start.7 = (f32[128,4]{0,1:T(4,128)S(1)}, f32[128,4]{0,1:T(4,128)}, u32[]{:S(2)}) copy-start(f32[128,4]{0,1:T(4,128)} %param.33) | copy-start | bytes 6148
Sparse Core Ops, SparseCore 0:
  86.9 31.4 all-gather.7
  120.2 50.7 all-gather.9
  196.1 26.7 all-gather.5
  227.8 26.6 reduce-scatter.1

commit v2 on v1

--- a/solution.py
+++ b/solution.py
@@ -370,18 +370,413 @@
     )(fq, fk, fv, gf, hq, hk, hv, gh, res, wf, wh, gain, eg, eu)
 
 
-def build_picks(route_rows, experts_count, capacity):
-    flat_routes = route_rows.reshape(-1)
-    onehot = (flat_routes[:, None] == jnp.arange(experts_count, dtype=jnp.int32)[None, :]).astype(
-        jnp.int32
+REL = (0, -1, 1, -2, 2, -3, 3, 4)
+AT = {r: i for i, r in enumerate(REL)}
+AT[-4] = AT[4]
+
+
+class Exchange:
+    def __init__(self, src, dst, relay, send, recv, rsend, rrecv):
+        self.src, self.dst, self.rl = src, dst, relay
+        self.send, self.recv, self.rsend, self.rrecv = send, recv, rsend, rrecv
+        s, y, z, x, c = position()
+        self.core = (c, 1 - c)
+        self.dev = lambda d, core: (sp_of(z, x + d, core), y)
+
+    def direct(self, g, d, crel):
+        m = d * 2 + crel
+        slot = ((4 - d) % 4) * 2 + crel
+        if d == 2:
+            return pltpu.make_async_remote_copy(
+                src_ref=self.src.at[pl.ds(g * 128 + 16 * m, 16)],
+                dst_ref=self.rl.at[g, crel],
+                send_sem=self.send.at[g, m],
+                recv_sem=self.rrecv.at[g, crel],
+                device_id=self.dev(1 if crel == 0 else 3, self.core[0]),
+                device_id_type=MESH,
+            )
+        return pltpu.make_async_remote_copy(
+            src_ref=self.src.at[pl.ds(g * 128 + 16 * m, 16)],
+            dst_ref=self.dst.at[pl.ds(g * 128 + 16 * slot, 16)],
+            send_sem=self.send.at[g, m],
+            recv_sem=self.recv.at[g, slot],
+            device_id=self.dev(d, self.core[crel]),
+            device_id_type=MESH,
+        )
+
+    def passed(self, g, crel):
+        slot = 4 + crel
+        return pltpu.make_async_remote_copy(
+            src_ref=self.rl.at[g, crel],
+            dst_ref=self.dst.at[pl.ds(g * 128 + 16 * slot, 16)],
+            send_sem=self.rsend.at[g, crel],
+            recv_sem=self.recv.at[g, slot],
+            device_id=self.dev(1 if crel == 0 else 3, self.core[crel]),
+            device_id_type=MESH,
+        )
+
+    def local(self, g):
+        return pltpu.make_async_copy(
+            self.src.at[pl.ds(g * 128, 16)],
+            self.dst.at[pl.ds(g * 128, 16)],
+            self.recv.at[g, 0],
+        )
+
+    def start(self, g):
+        for d, crel in ((2, 0), (2, 1), (1, 0), (3, 0), (1, 1), (3, 1), (0, 1)):
+            self.direct(g, d, crel).start()
+        self.local(g).start()
+
+    def relay(self, g):
+        for crel in (0, 1):
+            self.direct(g, 2, crel).wait_recv()
+            self.passed(g, crel).start()
+
+    def arrived(self, g):
+        self.local(g).wait()
+        for d, crel in ((0, 1), (1, 0), (3, 0), (1, 1), (3, 1)):
+            self.direct(g, d, crel).wait_recv()
+        for crel in (0, 1):
+            self.passed(g, crel).wait_recv()
+
+    def sent(self, g):
+        for d, crel in ((2, 0), (2, 1), (1, 0), (3, 0), (1, 1), (3, 1), (0, 1)):
+            self.direct(g, d, crel).wait_send()
+        for crel in (0, 1):
+            self.passed(g, crel).wait_send()
+
+
+def experts_kernel(
+    normed, middle, tile, gate_g, up_g, eg, eu, ed, sg, su, sd,
+    out,
+    tiles, tok, sel, wts, sb, xr, yb, yr, rl0, rl1, pz, zr, gu, dn, hid, sgv, suv, sdv, nall, spart, sin,
+    tile_send, tile_recv, ag_send, ag_recv, zs_send, zs_recv,
+    x_send, x_recv, xr_send, xr_recv, w_send, w_recv, s_send, s_recv, ld,
+):
+    s, y, z, x, c = position()
+    zup, zdown = (sp_of(z + 1, x, c), y), (sp_of(z - 1, x, c), y)
+    zs = [(sp_of(z + k, x, c), y) for k in range(1, 8)]
+    xs = [(sp_of(z, x + d, core), y) for d in (1, 3) for core in (c, 1 - c)]
+    sib = (s + 1 - 2 * c, y)
+    others = [(s, lax.rem(y + k, 4)) for k in (1, 2, 3)]
+    greet(zs + xs + [sib] + others)
+
+    loads = [
+        pltpu.make_async_copy(tile, tiles.at[z], ld.at[0]),
+        pltpu.make_async_copy(normed, tok.at[pl.ds(0, 32)], ld.at[1]),
+        pltpu.make_async_copy(normed, nall.at[y], ld.at[2]),
+        pltpu.make_async_copy(eg, gu.at[y, :, pl.ds(0, 128)], ld.at[3]),
+        pltpu.make_async_copy(eu, gu.at[y, :, pl.ds(128, 128)], ld.at[4]),
+        pltpu.make_async_copy(ed, dn.at[pl.ds(y * 128, 128)], ld.at[5]),
+        pltpu.make_async_copy(sg, sgv, ld.at[6]),
+        pltpu.make_async_copy(su, suv, ld.at[7]),
+        pltpu.make_async_copy(sd, sdv, ld.at[8]),
+    ]
+    for k in (1, 2, 3):
+        j = lax.rem(y + k, 4)
+        loads.append(pltpu.make_async_copy(gate_g.at[j], gu.at[j, :, pl.ds(0, 128)], ld.at[7 + 2 * k]))
+        loads.append(
+            pltpu.make_async_copy(up_g.at[j], gu.at[j, pl.ds(0, 2048), pl.ds(128, 128)], ld.at[8 + 2 * k])
+        )
+    for copy in loads:
+        copy.start()
+
+    loads[0].wait()
+
+    def tile_copy(k):
+        return pltpu.make_async_remote_copy(
+            src_ref=tiles.at[z],
+            dst_ref=tiles.at[z],
+            send_sem=tile_send.at[k - 1],
+            recv_sem=tile_recv.at[k - 1],
+            device_id=zs[k - 1],
+            device_id_type=MESH,
+        )
+
+    for k in range(1, 8):
+        tile_copy(k).start()
+
+    def ag(way, k, h):
+        sign = -1 if way == 0 else 1
+        return pltpu.make_async_remote_copy(
+            src_ref=tok.at[pl.ds(32 * AT[sign * (k - 1)] + 16 * h, 16)],
+            dst_ref=tok.at[pl.ds(32 * AT[sign * k] + 16 * h, 16)],
+            send_sem=ag_send.at[way, k - 1, h],
+            recv_sem=ag_recv.at[way, k - 1, h],
+            device_id=zup if way == 0 else zdown,
+            device_id_type=MESH,
+        )
+
+    def hops(way, k):
+        return (0, 1) if k < 4 else ((0,) if way == 0 else (1,))
+
+    loads[1].wait()
+    for h in (0, 1):
+        for way in (0, 1):
+            ag(way, 1, h).start()
+
+    ups = YGather(
+        [eu.at[pl.ds(2048 + h * 1024, 1024)] for h in (0, 1)],
+        lambda j, h: gu.at[j, pl.ds(2048 + h * 1024, 1024), pl.ds(128, 128)],
+        w_send.at[0], w_recv.at[0],
     )
-    earlier = jnp.cumsum(onehot, axis=0) - onehot
-    slot_rank = jnp.sum(earlier * onehot, axis=1)
-    slot_ids = flat_routes * capacity + slot_rank
-    picked = slot_ids[:, None] == jnp.arange(experts_count * capacity, dtype=jnp.int32)[None, :]
-    return picked.astype(jnp.bfloat16).reshape(
-        route_rows.shape[0], route_rows.shape[1], experts_count * capacity
+    downs = YGather(
+        [ed.at[pl.ds(h * 64, 64)] for h in (0, 1)],
+        lambda j, h: dn.at[pl.ds(j * 128 + h * 64, 64)],
+        w_send.at[1], w_recv.at[1],
     )
+    ups.start()
+    downs.start()
+
+    for k in range(1, 8):
+        tile_copy(k).wait_recv()
+
+    lane = lax.broadcasted_iota(jnp.int32, (4, 128), 1) // 32
+    row16 = lax.broadcasted_iota(jnp.int32, (16, 128), 0)
+    lane16 = lax.broadcasted_iota(jnp.int32, (16, 128), 1) // 32
+    r0 = lax.broadcasted_iota(jnp.int32, (128, 128), 0)
+    r1 = lax.broadcasted_iota(jnp.int32, (128, 128), 1)
+    earlier = jnp.where((r0 // 32 == r1 // 32) & (r0 < r1), 1.0, 0.0).astype(BF)
+
+    def picks(g):
+        names = jnp.zeros((4, 128), F32)
+        scale = jnp.zeros((4, 128), F32)
+        for i in range(4):
+            src = lax.rem(z + REL[g * 4 + i] + 8, 8)
+            names = jnp.where(lane == i, tiles[src, 0:4], names)
+            scale = jnp.where(lane == i, tiles[src, 4:8], scale)
+        occ, wrow = [], []
+        for d in range(4):
+            for crel in (0, 1):
+                core = c + crel - 2 * c * crel
+                expert = (z * 8 + lax.rem(x + d, 4) * 2 + core).astype(F32)
+                hit = jnp.where(names == expert, 1.0, 0.0)
+                occ.append(jnp.sum(hit, axis=0, keepdims=True))
+                wrow.append(jnp.sum(hit * scale, axis=0, keepdims=True))
+        occupied = jnp.concatenate(occ, axis=0)
+        rank = jnp.dot(occupied.astype(BF), earlier, preferred_element_type=F32)
+        weighted = []
+        for m in range(8):
+            chosen = (
+                (lane16 == row16 // 4)
+                & (rank[m : m + 1] == (row16 % 4).astype(F32))
+                & (occ[m] > 0.5)
+            )
+            sel[g, pl.ds(16 * m, 16)] = jnp.where(chosen, 1.0, 0.0).astype(BF)
+            weighted.append(jnp.where(chosen, wrow[m], 0.0))
+        full = jnp.concatenate(weighted, axis=0).T
+        high = full.astype(BF)
+        wts[g, 0] = high
+        wts[g, 1] = (full - high.astype(F32)).astype(BF)
+
+    fwd = Exchange(sb, xr, rl0, x_send.at[0], x_recv.at[0], xr_send.at[0], xr_recv.at[0])
+    back = Exchange(yb, yr, rl1, x_send.at[1], x_recv.at[1], xr_send.at[1], xr_recv.at[1])
+
+    def select(g):
+        for n in range(4):
+            cols = slice(n * 1024, (n + 1) * 1024)
+            sb[g * 128 : (g + 1) * 128, cols] = jnp.dot(
+                sel[g], tok[g * 128 : (g + 1) * 128, cols], preferred_element_type=F32
+            ).astype(BF)
+        fwd.start(g)
+
+    picks(0)
+    picks(1)
+    for k in range(1, 5):
+        for h in (0, 1):
+            for way in (0, 1):
+                if h in hops(way, k):
+                    ag(way, k, h).wait_recv()
+                    if k < 4 and h in hops(way, k + 1):
+                        ag(way, k + 1, h).start()
+        if k == 2:
+            select(0)
+            ups.relay()
+        if k == 3:
+            fwd.relay(0)
+    select(1)
+    downs.relay()
+
+    def rows(k):
+        return pltpu.make_async_remote_copy(
+            src_ref=nall.at[y],
+            dst_ref=nall.at[y],
+            send_sem=s_send.at[0, k - 1],
+            recv_sem=s_recv.at[0, k - 1],
+            device_id=others[k - 1],
+            device_id_type=MESH,
+        )
+
+    loads[2].wait()
+    for k in (2, 1, 3):
+        rows(k).start()
+
+    fwd.relay(1)
+    for copy in loads[3:]:
+        copy.wait()
+    ups.finish()
+    fwd.arrived(0)
+    fwd.arrived(1)
+
+    @pl.loop(0, 4)
+    def _(j):
+        both = jnp.dot(xr[...], gu[j], preferred_element_type=F32)
+        g, u = both[:, 0:128], both[:, 128:256]
+        hid[:, pl.ds(pl.multiple_of(j * 128, 128), 128)] = (g / (1.0 + jnp.exp(-g)) * u).astype(BF)
+
+    downs.finish()
+
+    @pl.loop(0, 4)
+    def _(n):
+        cols = pl.ds(pl.multiple_of(n * 1024, 1024), 1024)
+        yb[:, cols] = jnp.dot(hid[...], dn[:, cols], preferred_element_type=F32).astype(BF)
+
+    back.start(1)
+    back.start(0)
+
+    for k in (2, 1, 3):
+        rows(k).wait_recv()
+    everyone = nall[...].reshape(128, D)
+    g = jnp.dot(everyone, sgv[...], preferred_element_type=F32)
+    u = jnp.dot(everyone, suv[...], preferred_element_type=F32)
+    shared_hidden = (g / (1.0 + jnp.exp(-g)) * u).astype(BF)
+    for n in range(4):
+        cols = slice(n * 1024, (n + 1) * 1024)
+        spart[:, :, cols] = (
+            jnp.dot(shared_hidden, sdv[:, cols], preferred_element_type=F32).astype(BF).reshape(4, 32, 1024)
+        )
+
+    def share(k):
+        return pltpu.make_async_remote_copy(
+            src_ref=spart.at[lax.rem(y + k, 4)],
+            dst_ref=sin.at[k - 1],
+            send_sem=s_send.at[1, k - 1],
+            recv_sem=s_recv.at[1, k - 1],
+            device_id=others[k - 1],
+            device_id_type=MESH,
+        )
+
+    for k in (2, 1, 3):
+        share(k).start()
+
+    back.relay(1)
+    back.relay(0)
+
+    def combine(g):
+        back.arrived(g)
+        for n in range(4):
+            cols = slice(n * 1024, (n + 1) * 1024)
+            pz[g * 128 : (g + 1) * 128, cols] = (
+                jnp.dot(wts[g, 0], yr[g * 128 : (g + 1) * 128, cols], preferred_element_type=F32)
+                + jnp.dot(wts[g, 1], yr[g * 128 : (g + 1) * 128, cols], preferred_element_type=F32)
+            ).astype(BF)
+
+    def zsum(way, m, h):
+        sign = 1 if way == 0 else -1
+        return pltpu.make_async_remote_copy(
+            src_ref=pz.at[pl.ds(32 * AT[sign * m] + 16 * h, 16)],
+            dst_ref=zr.at[way, m - 1, pl.ds(16 * h, 16)],
+            send_sem=zs_send.at[way, m - 1, h],
+            recv_sem=zs_recv.at[way, m - 1, h],
+            device_id=zup if way == 0 else zdown,
+            device_id_type=MESH,
+        )
+
+    def add_and_send(m):
+        for h in (0, 1):
+            for way in (0, 1):
+                if h not in hops(way, m):
+                    continue
+                sign = 1 if way == 0 else -1
+                if m < 4 and h in hops(way, m + 1):
+                    zsum(way, m + 1, h).wait_recv()
+                    at = slice(32 * AT[sign * m] + 16 * h, 32 * AT[sign * m] + 16 * h + 16)
+                    pz[at] = (
+                        pz[at].astype(F32) + zr[way, m, 16 * h : 16 * h + 16].astype(F32)
+                    ).astype(BF)
+                zsum(way, m, h).start()
+
+    combine(1)
+    add_and_send(4)
+    add_and_send(3)
+    combine(0)
+    add_and_send(2)
+    add_and_send(1)
+
+    for k in (2, 1, 3):
+        share(k).wait_recv()
+    for h in (0, 1):
+        for way in (0, 1):
+            zsum(way, 1, h).wait_recv()
+    for n in range(4):
+        cols = slice(n * 1024, (n + 1) * 1024)
+        total = middle[:, cols] + spart[y, :, cols].astype(F32)
+        for k in range(3):
+            total = total + sin[k, :, cols].astype(F32)
+        total = total + pz[0:32, cols].astype(F32)
+        total = total + zr[0, 0, :, cols].astype(F32) + zr[1, 0, :, cols].astype(F32)
+        out[:, cols] = total.astype(BF)
+
+    for k in range(1, 8):
+        tile_copy(k).wait_send()
+    for k in range(1, 5):
+        for way in (0, 1):
+            for h in hops(way, k):
+                ag(way, k, h).wait_send()
+                zsum(way, k, h).wait_send()
+    for g in (0, 1):
+        fwd.sent(g)
+        back.sent(g)
+    for k in (1, 2, 3):
+        rows(k).wait_send()
+        share(k).wait_send()
+
+
+def experts(normed, middle, tile, gate_g, up_g, eg, eu, ed, sg, su, sd):
+    vmem = pl.BlockSpec(memory_space=pltpu.VMEM)
+    anym = pl.BlockSpec(memory_space=pl.ANY)
+    dma = pltpu.SemaphoreType.DMA
+    return pl.pallas_call(
+        experts_kernel,
+        name="experts",
+        out_shape=jax.ShapeDtypeStruct((32, D), BF),
+        in_specs=[anym, vmem] + [anym] * 9,
+        out_specs=vmem,
+        scratch_shapes=[
+            pltpu.VMEM((8, 8, 128), F32),
+            pltpu.VMEM((256, D), BF),
+            pltpu.VMEM((2, 128, 128), BF),
+            pltpu.VMEM((2, 2, 128, 128), BF),
+            pltpu.VMEM((256, D), BF),
+            pltpu.VMEM((256, D), BF),
+            pltpu.VMEM((256, D), BF),
+            pltpu.VMEM((256, D), BF),
+            pltpu.VMEM((2, 2, 16, D), BF),
+            pltpu.VMEM((2, 2, 16, D), BF),
+            pltpu.VMEM((256, D), BF),
+            pltpu.VMEM((2, 4, 32, D), BF),
+            pltpu.VMEM((4, 4096, 256), BF),
+            pltpu.VMEM((512, D), BF),
+            pltpu.VMEM((256, 512), BF),
+            pltpu.VMEM((4096, 128), BF),
+            pltpu.VMEM((4096, 128), BF),
+            pltpu.VMEM((128, D), BF),
+            pltpu.VMEM((4, 32, D), BF),
+            pltpu.VMEM((4, 32, D), BF),
+            pltpu.VMEM((3, 32, D), BF),
+            dma((7,)), dma((7,)),
+            dma((2, 4, 2)), dma((2, 4, 2)),
+            dma((2, 4, 2)), dma((2, 4, 2)),
+            dma((2, 2, 8)), dma((2, 2, 8)),
+            dma((2, 2, 2)), dma((2, 2, 2)),
+            dma((2, 6)), dma((2, 6)),
+            dma((2, 3)), dma((2, 3)),
+            dma((15,)),
+        ],
+        compiler_params=pltpu.CompilerParams(
+            collective_id=1, has_side_effects=True, vmem_limit_bytes=60 * 1024 * 1024
+        ),
+    )(normed, middle, tile, gate_g, up_g, eg, eu, ed, sg, su, sd)
 
 
 def body(
@@ -390,40 +785,17 @@
     expert_gate, expert_up, expert_down, shared_gate, shared_up, shared_down,
 ):
     quarter = lax.axis_index("tp")
-    middle, normed_own, gates_g, ups_g = attend(
+    own = lambda a: lax.dynamic_slice_in_dim(a.T.astype(F32), quarter * 32, 32, 1)
+    tile = jnp.tile(jnp.concatenate([own(routes), own(route_weights)], axis=0), (1, 4))
+    middle, normed, gates, ups = attend(
         full_queries, full_keys, full_values, full_gates.T, half_queries, half_keys, half_values,
         half_gates.T, residual, full_output, half_output, norm_gain.reshape(1, D),
         expert_gate[0], expert_up[0],
     )
-    own_g = lax.dynamic_update_slice(gates_g, expert_gate, (quarter, 0, 0))
-    own_u = lax.dynamic_update_slice(ups_g, expert_up[:, :2048], (quarter, 0, 0))
-    whole_gate = jnp.moveaxis(own_g, 0, 1).reshape(4096, 512)
-    up_top = jnp.moveaxis(own_u, 0, 1).reshape(2048, 512)
-    up_bot = lax.all_gather(expert_up[0, 2048:], "tp", axis=1, tiled=True)
-    whole_up = jnp.concatenate([up_top, up_bot], 0)
-    whole_down = lax.all_gather(expert_down[0], "tp", axis=0, tiled=True)
-    normed = lax.all_gather(normed_own, "tp", axis=0, tiled=True)
-    shared_hidden = (
-        jax.nn.silu(jnp.dot(normed, shared_gate, preferred_element_type=F32))
-        * jnp.dot(normed, shared_up, preferred_element_type=F32)
-    ).astype(BF)
-    shared_term = jnp.dot(shared_hidden, shared_down, preferred_element_type=F32).reshape(4, 32, D)
-    own_routes = lax.dynamic_slice_in_dim(routes, quarter * 32, 32, 0)
-    own_picks = build_picks(own_routes, 64, 4)
-    occupancy = jnp.sum(own_picks, axis=1)
-    buffer_rows = jnp.einsum("ts,td->sd", occupancy, normed_own, preferred_element_type=F32).astype(BF)
-    received = lax.all_to_all(buffer_rows.reshape(64, 4, D), "sp", split_axis=0, concat_axis=0, tiled=True)
-    flat_rows = received.reshape(-1, D)
-    gate_part = jnp.dot(flat_rows, whole_gate, preferred_element_type=F32)
-    up_part = jnp.dot(flat_rows, whole_up, preferred_element_type=F32)
-    hidden = (jax.nn.silu(gate_part) * up_part).astype(BF)
-    finished = jnp.dot(hidden, whole_down, preferred_element_type=F32).astype(BF).reshape(64, 4, D)
-    summed = lax.psum_scatter(shared_term.astype(BF), "tp", scatter_dimension=0, tiled=True).astype(F32)[0]
-    returned = lax.all_to_all(finished, "sp", split_axis=0, concat_axis=0, tiled=True)
-    gathered = jnp.einsum("tks,sd->tkd", own_picks, returned.reshape(256, D), preferred_element_type=F32)
-    own_weights = lax.dynamic_slice_in_dim(route_weights, quarter * 32, 32, 0)
-    routed = jnp.sum(own_weights[..., None] * gathered, axis=1)
-    return (middle + summed + routed).astype(BF)
+    return experts(
+        normed, middle, tile, gates, ups, expert_gate[0], expert_up[0], expert_down[0],
+        shared_gate, shared_up, shared_down,
+    )
 
 
 def solution(mesh):

time: 264 us -> 193 us (0.73)
  Pallas kernels: 78.3 us -> 187 us
  waiting for transfers between devices: 104 us -> 0 us
  local copies, waits for them, and re-layouts: 26 us -> 3.1 us
  matrix products: 19.3 us -> 0 us
  starting transfers between devices: 19.3 us -> 0 us
  between operations: 13.3 us -> 0.02 us
    pallas_call x0 -> x1, Pallas kernels: none -> 109 us  [experts(): pl.pallas_call(experts_kernel, name='experts', out_shape=jax.ShapeDtypeSt...]
    all_to_all x2 -> x0, waiting for transfers between devices: 55.4 us -> none  [the longest x1 38.6 us: body(): lax.all_to_all(buffer_rows.reshape(64, 4, D), 'sp', split_axis=0, concat_...]
    all_gather x3 -> x0, waiting for transfers between devices: 41.4 us -> none  [the longest x1 28.7 us: body(): normed = lax.all_gather(normed_own, 'tp', axis=0, tiled=True)]
    dot_general x6 -> x0, matrix products: 19.3 us -> none  [the longest x1 7.43 us: body(): jnp.dot(hidden, whole_down, preferred_element_type=F32).astype(BF)]
    all_to_all x2 -> x0, starting transfers between devices: 19.2 us -> none  [the longest x1 10.8 us: body(): lax.all_to_all(finished, 'sp', split_axis=0, concat_axis=0, tiled=True)]
    reshape x4 -> x0, local copies, waits for them, and re-layouts: 10.9 us -> none  [the longest x1 4.09 us: body(): jnp.dot(hidden, whole_down, preferred_element_type=F32).astype(BF)]
    transpose x2 -> x0, local copies, waits for them, and re-layouts: 10.4 us -> none  [the longest x1 6.41 us: body(): whole_gate = jnp.moveaxis(own_g, 0, 1).reshape(4096, 512)]
    reduce_scatter x1 -> x0, waiting for transfers between devices: 6.06 us -> none  [body(): lax.psum_scatter(shared_term.astype(BF), 'tp', scatter_dimension=0, tiled...]
  transfers between devices with their start and end apart: 6 -> 0, of which waited for: 5 -> 0; matrix products, arithmetic and copies ran while one was open for 12% -> 0% of each run, Pallas kernels for 0% -> 0%
where the time goes in v2:
time: 193 us; the launch traced here: 191 us
  Pallas kernels  187 us (97%)
  local copies, waits for them, and re-layouts  3.1 us (2%)
    pallas_call x1, Pallas kernels, experts(): pl.pallas_call(experts_kernel, name='experts', out_shape=jax.ShapeDtypeSt...  109 us
    pallas_call x1, Pallas kernels, attend(): pl.pallas_call(attend_kernel, name='attend', out_shape=(jax.ShapeDtypeStr...  78.2 us

profile of v2, /device:TPU:2, one launch (start us, length us, event | category | flops | bytes accessed | tf_op | source)
XLA Modules:
  0.0 191.3 jit_solution(147014973655778253)
XLA Ops:
  0.0 0.7 convert_element_type.4
  0.7 0.8 dynamic-slice_bitcast_fusion
  1.5 0.7 tile.10
  2.1 78.2 %attend.1 = (f32[32,4096]{1,0:T(8,128)}, bf16[32,4096]{1,0:T(8,128)(2,1)}, bf16[4,4096,128]{2,1,0:T(8,128)(2,1)}, bf16[4,2048,128]{2,1,0:T(8,128)(2,1)}) custom-call(bf16[128,256]{1,0:T(8,128)(2,1)} %fq.1, bf16[128,128]{1,0:T(8,128)(2,1)} %fk.1, bf16[128,128]{1,0:T(8,128)(2,1)} %fv.1, f32[2,8192]{1,0:T(2,128)} %bitcast.16, bf16[128,256]{1,0:T(8,128)(2,1)} %hq.1, ...), custom_call_target="tpu_custom_call" | custom-call | tf_op jit(solution)/shard_map/attend/pallas_call | solution.py:336
  80.4 109.2 %experts.1 = bf16[32,4096]{1,0:T(8,128)(2,1)} custom-call(bf16[32,4096]{1,0:T(8,128)(2,1)} %get-tuple-element.9.normed, f32[32,4096]{1,0:T(8,128)} %get-tuple-element.10.middle, f32[8,128]{1,0:T(8,128)} %tile.10, bf16[4,4096,128]{2,1,0:T(8,128)(2,1)} %get-tuple-element.11.gate_g, bf16[4,2048,128]{2,1,0:T(8,128)(2,1)} %get-tuple-element.12.up_g, ...), custom_call_target="tpu_custom_call" | custom-call | tf_op jit(solution)/shard_map/experts/pallas_call | solution.py:739
  189.6 1.7 copy.22
  (2 shorter events, 0.0 us)

commit v3 on v2

--- a/solution.py
+++ b/solution.py
@@ -145,10 +145,63 @@
         self.copy(1, above, 1, 1).wait_send()
 
 
+class YReduce:
+    def __init__(self, part, far, near, send_sem, recv_sem, width):
+        s, y, *_ = position()
+        self.part, self.far, self.near = part, far, near
+        self.send, self.recv, self.width = send_sem, recv_sem, width
+        self.next = (lax.rem(y + 1, 4), lax.rem(y + 3, 4))
+        self.across = lax.rem(y + 2, 4)
+        self.dev = [(s, self.next[0]), (s, self.next[1])]
+
+    def copy(self, n, way, kind):
+        cols = pl.ds(n * self.width, self.width)
+        low, high = pl.ds(0, 16), pl.ds(16, 16)
+        merged, plain = (high, low) if way == 0 else (low, high)
+        if kind == 0:
+            src, dst = self.part.at[self.across, merged, cols], self.far.at[way, :, cols]
+        else:
+            rows = plain if kind == 1 else merged
+            src, dst = self.part.at[self.next[way], rows, cols], self.near.at[way, rows, cols]
+        return pltpu.make_async_remote_copy(
+            src_ref=src,
+            dst_ref=dst,
+            send_sem=self.send.at[n, way, kind],
+            recv_sem=self.recv.at[n, way, kind],
+            device_id=self.dev[way],
+            device_id_type=MESH,
+        )
+
+    def start(self, n):
+        for kind in (0, 1):
+            for way in (0, 1):
+                self.copy(n, way, kind).start()
+
+    def relay(self, n):
+        cols = pl.ds(n * self.width, self.width)
+        for way in (0, 1):
+            rows = pl.ds(16, 16) if way == 0 else pl.ds(0, 16)
+            self.copy(n, way, 0).wait_recv()
+            self.part[self.next[way], rows, cols] = (
+                self.part[self.next[way], rows, cols].astype(F32) + self.far[way, :, cols].astype(F32)
+            ).astype(BF)
+            self.copy(n, way, 2).start()
+
+    def arrived(self, n):
+        for kind in (1, 2):
+            for way in (0, 1):
+                self.copy(n, way, kind).wait_recv()
+
+    def sent(self, n):
+        for kind in (0, 1, 2):
+            for way in (0, 1):
+                self.copy(n, way, kind).wait_send()
+
+
 def attend_kernel(
     fq, fk, fv, gf, hq, hk, hv, gh, res, wf, wh, gain, eg, eu,
     mid_out, norm_out, gate_out, up_out,
-    kva, kvb, qs, acc, mx, tot, att, part, inbox, resv,
+    kva, kvb, qs, acc, mx, tot, att, part, far, near, resv,
     own_sem, kv_send, kv_recv, w_send, w_recv, rs_send, rs_recv, res_sem,
 ):
     s, y, z, x, c = position()
@@ -291,40 +344,30 @@
     gates.finish()
     ups.finish()
 
-    def share(k, n, device):
-        return pltpu.make_async_remote_copy(
-            src_ref=part.at[lax.rem(y + k, 4), :, pl.ds(n * 1024, 1024)],
-            dst_ref=inbox.at[k - 1, :, pl.ds(n * 1024, 1024)],
-            send_sem=rs_send.at[k - 1, n],
-            recv_sem=rs_recv.at[k - 1, n],
-            device_id=device,
-            device_id_type=MESH,
-        )
-
+    sums = YReduce(part, far, near, rs_send, rs_recv, 1024)
     for n in range(4):
         cols = slice(n * 1024, (n + 1) * 1024)
         product = jnp.dot(att[:, 0:256], wf[:, cols], preferred_element_type=F32) + jnp.dot(
             att[:, 256:512], wh[:, cols], preferred_element_type=F32
         )
         part[:, :, cols] = product.astype(BF).reshape(4, 32, 1024)
-        for k, device in zip((2, 1, 3), others):
-            share(k, n, device).start()
+        sums.start(n)
+    for n in range(4):
+        sums.relay(n)
     res_copy.wait()
     square = jnp.zeros((32, 1), F32)
     for n in range(4):
         cols = slice(n * 1024, (n + 1) * 1024)
         total = resv[:, cols].astype(F32) + part[y, :, cols].astype(F32)
-        for k, device in zip((2, 1, 3), others):
-            share(k, n, device).wait_recv()
-            total = total + inbox[k - 1, :, cols].astype(F32)
+        sums.arrived(n)
+        total = total + near[0, :, cols].astype(F32) + near[1, :, cols].astype(F32)
         mid_out[:, cols] = total
         square = square + jnp.sum(total * total, axis=1, keepdims=True)
     factor = lax.rsqrt(square * (1.0 / D) + 1e-06)
     norm_out[...] = (mid_out[...] * factor * gain[...]).astype(BF)
 
     for n in range(4):
-        for k, device in zip((2, 1, 3), others):
-            share(k, n, device).wait_send()
+        sums.sent(n)
     for prt in (0, 1):
         everything = kv[prt].at[pl.ds(0, 63)]
         pltpu.make_async_copy(everything, everything, kv_send.at[prt]).wait()
@@ -353,15 +396,16 @@
             pltpu.VMEM((3, 256, 128), F32),
             pltpu.VMEM((128, 512), BF),
             pltpu.VMEM((4, 32, D), BF),
-            pltpu.VMEM((3, 32, D), BF),
+            pltpu.VMEM((2, 16, D), BF),
+            pltpu.VMEM((2, 32, D), BF),
             pltpu.VMEM((32, D), BF),
             pltpu.SemaphoreType.DMA((4,)),
             pltpu.SemaphoreType.DMA((2,)),
             pltpu.SemaphoreType.DMA((2, 64)),
             pltpu.SemaphoreType.DMA((2, 6)),
             pltpu.SemaphoreType.DMA((2, 6)),
-            pltpu.SemaphoreType.DMA((3, 4)),
-            pltpu.SemaphoreType.DMA((3, 4)),
+            pltpu.SemaphoreType.DMA((4, 2, 3)),
+            pltpu.SemaphoreType.DMA((4, 2, 3)),
             pltpu.SemaphoreType.DMA,
         ],
         compiler_params=pltpu.CompilerParams(
@@ -376,82 +420,86 @@
 
 
 class Exchange:
-    def __init__(self, src, dst, relay, send, recv, rsend, rrecv):
+    def __init__(self, src, dst, relay, send, recv, rsend, rrecv, width):
+        self.width = width
         self.src, self.dst, self.rl = src, dst, relay
         self.send, self.recv, self.rsend, self.rrecv = send, recv, rsend, rrecv
         s, y, z, x, c = position()
         self.core = (c, 1 - c)
         self.dev = lambda d, core: (sp_of(z, x + d, core), y)
 
-    def direct(self, g, d, crel):
+    def direct(self, g, d, crel, n=0):
+        cols = pl.ds(n * self.width, self.width)
         m = d * 2 + crel
         slot = ((4 - d) % 4) * 2 + crel
         if d == 2:
             return pltpu.make_async_remote_copy(
-                src_ref=self.src.at[pl.ds(g * 128 + 16 * m, 16)],
-                dst_ref=self.rl.at[g, crel],
-                send_sem=self.send.at[g, m],
-                recv_sem=self.rrecv.at[g, crel],
+                src_ref=self.src.at[pl.ds(g * 128 + 16 * m, 16), cols],
+                dst_ref=self.rl.at[g, crel, :, cols],
+                send_sem=self.send.at[n, g, m],
+                recv_sem=self.rrecv.at[n, g, crel],
                 device_id=self.dev(1 if crel == 0 else 3, self.core[0]),
                 device_id_type=MESH,
             )
         return pltpu.make_async_remote_copy(
-            src_ref=self.src.at[pl.ds(g * 128 + 16 * m, 16)],
-            dst_ref=self.dst.at[pl.ds(g * 128 + 16 * slot, 16)],
-            send_sem=self.send.at[g, m],
-            recv_sem=self.recv.at[g, slot],
+            src_ref=self.src.at[pl.ds(g * 128 + 16 * m, 16), cols],
+            dst_ref=self.dst.at[pl.ds(g * 128 + 16 * slot, 16), cols],
+            send_sem=self.send.at[n, g, m],
+            recv_sem=self.recv.at[n, g, slot],
             device_id=self.dev(d, self.core[crel]),
             device_id_type=MESH,
         )
 
-    def passed(self, g, crel):
+    def passed(self, g, crel, n=0):
+        cols = pl.ds(n * self.width, self.width)
         slot = 4 + crel
         return pltpu.make_async_remote_copy(
-            src_ref=self.rl.at[g, crel],
-            dst_ref=self.dst.at[pl.ds(g * 128 + 16 * slot, 16)],
-            send_sem=self.rsend.at[g, crel],
-            recv_sem=self.recv.at[g, slot],
+            src_ref=self.rl.at[g, crel, :, cols],
+            dst_ref=self.dst.at[pl.ds(g * 128 + 16 * slot, 16), cols],
+            send_sem=self.rsend.at[n, g, crel],
+            recv_sem=self.recv.at[n, g, slot],
             device_id=self.dev(1 if crel == 0 else 3, self.core[crel]),
             device_id_type=MESH,
         )
 
-    def local(self, g):
+    def local(self, g, n=0):
+        cols = pl.ds(n * self.width, self.width)
         return pltpu.make_async_copy(
-            self.src.at[pl.ds(g * 128, 16)],
-            self.dst.at[pl.ds(g * 128, 16)],
-            self.recv.at[g, 0],
-        )
-
-    def start(self, g):
+            self.src.at[pl.ds(g * 128, 16), cols],
+            self.dst.at[pl.ds(g * 128, 16), cols],
+            self.recv.at[n, g, 0],
+        )
+
+    def start(self, g, n=0):
         for d, crel in ((2, 0), (2, 1), (1, 0), (3, 0), (1, 1), (3, 1), (0, 1)):
-            self.direct(g, d, crel).start()
-        self.local(g).start()
-
-    def relay(self, g):
+            self.direct(g, d, crel, n).start()
+        self.local(g, n).start()
+
+    def relay(self, g, n=0):
         for crel in (0, 1):
-            self.direct(g, 2, crel).wait_recv()
-            self.passed(g, crel).start()
-
-    def arrived(self, g):
-        self.local(g).wait()
+            self.direct(g, 2, crel, n).wait_recv()
+            self.passed(g, crel, n).start()
+
+    def arrived(self, g, n=0):
+        self.local(g, n).wait()
         for d, crel in ((0, 1), (1, 0), (3, 0), (1, 1), (3, 1)):
-            self.direct(g, d, crel).wait_recv()
+            self.direct(g, d, crel, n).wait_recv()
         for crel in (0, 1):
-            self.passed(g, crel).wait_recv()
-
-    def sent(self, g):
+            self.passed(g, crel, n).wait_recv()
+
+    def sent(self, g, n=0):
         for d, crel in ((2, 0), (2, 1), (1, 0), (3, 0), (1, 1), (3, 1), (0, 1)):
-            self.direct(g, d, crel).wait_send()
+            self.direct(g, d, crel, n).wait_send()
         for crel in (0, 1):
-            self.passed(g, crel).wait_send()
+            self.passed(g, crel, n).wait_send()
 
 
 def experts_kernel(
     normed, middle, tile, gate_g, up_g, eg, eu, ed, sg, su, sd,
     out,
-    tiles, tok, sel, wts, sb, xr, yb, yr, rl0, rl1, pz, zr, gu, dn, hid, sgv, suv, sdv, nall, spart, sin,
+    tiles, tok, sel, wts, sb, xr, yb, yr, rl0, rl1, pz, zr, gu, dn, hid, sgv, suv, sdv, nall, spart, sfar, snear,
     tile_send, tile_recv, ag_send, ag_recv, zs_send, zs_recv,
-    x_send, x_recv, xr_send, xr_recv, w_send, w_recv, s_send, s_recv, ld,
+    x_send, x_recv, xr_send, xr_recv, w_send, w_recv, g_send, g_recv, s_send, s_recv, ld,
 ):
     s, y, z, x, c = position()
     zup, zdown = (sp_of(z + 1, x, c), y), (sp_of(z - 1, x, c), y)
@@ -520,13 +568,23 @@
         lambda j, h: gu.at[j, pl.ds(2048 + h * 1024, 1024), pl.ds(128, 128)],
         w_send.at[0], w_recv.at[0],
     )
-    downs = YGather(
-        [ed.at[pl.ds(h * 64, 64)] for h in (0, 1)],
-        lambda j, h: dn.at[pl.ds(j * 128 + h * 64, 64)],
-        w_send.at[1], w_recv.at[1],
+    def down_chunk(n):
+        cols = pl.ds(n * 1024, 1024)
+        return YGather(
+            [ed.at[pl.ds(h * 64, 64), cols] for h in (0, 1)],
+            lambda j, h: dn.at[pl.ds(j * 128 + h * 64, 64), cols],
+            w_send.at[1 + n], w_recv.at[1 + n],
+        )
+
+    downs = [down_chunk(n) for n in range(4)]
+    rows = YGather(
+        [normed.at[pl.ds(h * 16, 16)] for h in (0, 1)],
+        lambda j, h: nall.at[j, pl.ds(h * 16, 16)],
+        g_send, g_recv,
     )
     ups.start()
-    downs.start()
+    downs[0].start()
+    downs[1].start()
 
     for k in range(1, 8):
         tile_copy(k).wait_recv()
@@ -569,8 +627,8 @@
         wts[g, 0] = high
         wts[g, 1] = (full - high.astype(F32)).astype(BF)
 
-    fwd = Exchange(sb, xr, rl0, x_send.at[0], x_recv.at[0], xr_send.at[0], xr_recv.at[0])
-    back = Exchange(yb, yr, rl1, x_send.at[1], x_recv.at[1], xr_send.at[1], xr_recv.at[1])
+    fwd = Exchange(sb, xr, rl0, x_send.at[pl.ds(0, 1)], x_recv.at[pl.ds(0, 1)], xr_send.at[pl.ds(0, 1)], xr_recv.at[pl.ds(0, 1)], D)
+    back = Exchange(yb, yr, rl1, x_send.at[pl.ds(1, 4)], x_recv.at[pl.ds(1, 4)], xr_send.at[pl.ds(1, 4)], xr_recv.at[pl.ds(1, 4)], 1024)
 
     def select(g):
         for n in range(4):
@@ -592,27 +650,18 @@
         if k == 2:
             select(0)
             ups.relay()
+            downs[2].start()
+            downs[3].start()
         if k == 3:
             fwd.relay(0)
+            downs[0].relay()
     select(1)
-    downs.relay()
-
-    def rows(k):
-        return pltpu.make_async_remote_copy(
-            src_ref=nall.at[y],
-            dst_ref=nall.at[y],
-            send_sem=s_send.at[0, k - 1],
-            recv_sem=s_recv.at[0, k - 1],
-            device_id=others[k - 1],
-            device_id_type=MESH,
-        )
-
-    loads[2].wait()
-    for k in (2, 1, 3):
-        rows(k).start()
+    downs[1].relay()
 
     fwd.relay(1)
-    for copy in loads[3:]:
+    downs[2].relay()
+    rows.start()
+    for copy in loads[2:]:
         copy.wait()
     ups.finish()
     fwd.arrived(0)
@@ -624,98 +673,103 @@
         g, u = both[:, 0:128], both[:, 128:256]
         hid[:, pl.ds(pl.multiple_of(j * 128, 128), 128)] = (g / (1.0 + jnp.exp(-g)) * u).astype(BF)
 
-    downs.finish()
-
-    @pl.loop(0, 4)
-    def _(n):
-        cols = pl.ds(pl.multiple_of(n * 1024, 1024), 1024)
+    sums = YReduce(spart, sfar, snear, s_send, s_recv, D)
+
+    def finish_rows(n):
+        downs[n].finish()
+        cols = slice(n * 1024, (n + 1) * 1024)
         yb[:, cols] = jnp.dot(hid[...], dn[:, cols], preferred_element_type=F32).astype(BF)
-
-    back.start(1)
-    back.start(0)
-
-    for k in (2, 1, 3):
-        rows(k).wait_recv()
-    everyone = nall[...].reshape(128, D)
-    g = jnp.dot(everyone, sgv[...], preferred_element_type=F32)
-    u = jnp.dot(everyone, suv[...], preferred_element_type=F32)
-    shared_hidden = (g / (1.0 + jnp.exp(-g)) * u).astype(BF)
-    for n in range(4):
-        cols = slice(n * 1024, (n + 1) * 1024)
-        spart[:, :, cols] = (
-            jnp.dot(shared_hidden, sdv[:, cols], preferred_element_type=F32).astype(BF).reshape(4, 32, 1024)
-        )
-
-    def share(k):
-        return pltpu.make_async_remote_copy(
-            src_ref=spart.at[lax.rem(y + k, 4)],
-            dst_ref=sin.at[k - 1],
-            send_sem=s_send.at[1, k - 1],
-            recv_sem=s_recv.at[1, k - 1],
-            device_id=others[k - 1],
-            device_id_type=MESH,
-        )
-
-    for k in (2, 1, 3):
-        share(k).start()
-
-    back.relay(1)
-    back.relay(0)
-
-    def combine(g):
-        back.arrived(g)
+        for g in (1, 0):
+            back.start(g, n)
+
+    def shared():
+        rows.finish()
+        everyone = nall[...].reshape(128, D)
+        g = jnp.dot(everyone, sgv[...], preferred_element_type=F32)
+        u = jnp.dot(everyone, suv[...], preferred_element_type=F32)
+        shared_hidden = (g / (1.0 + jnp.exp(-g)) * u).astype(BF)
         for n in range(4):
             cols = slice(n * 1024, (n + 1) * 1024)
+            spart[:, :, cols] = (
+                jnp.dot(shared_hidden, sdv[:, cols], preferred_element_type=F32)
+                .astype(BF)
+                .reshape(4, 32, 1024)
+            )
+        sums.start(0)
+
+    def combine(n):
+        cols = slice(n * 1024, (n + 1) * 1024)
+        for g in (1, 0):
+            back.arrived(g, n)
             pz[g * 128 : (g + 1) * 128, cols] = (
                 jnp.dot(wts[g, 0], yr[g * 128 : (g + 1) * 128, cols], preferred_element_type=F32)
                 + jnp.dot(wts[g, 1], yr[g * 128 : (g + 1) * 128, cols], preferred_element_type=F32)
             ).astype(BF)
 
-    def zsum(way, m, h):
+    def zsum(n, way, m, h):
         sign = 1 if way == 0 else -1
+        cols = pl.ds(n * 1024, 1024)
         return pltpu.make_async_remote_copy(
-            src_ref=pz.at[pl.ds(32 * AT[sign * m] + 16 * h, 16)],
-            dst_ref=zr.at[way, m - 1, pl.ds(16 * h, 16)],
-            send_sem=zs_send.at[way, m - 1, h],
-            recv_sem=zs_recv.at[way, m - 1, h],
+            src_ref=pz.at[pl.ds(32 * AT[sign * m] + 16 * h, 16), cols],
+            dst_ref=zr.at[way, m - 1, pl.ds(16 * h, 16), cols],
+            send_sem=zs_send.at[n, way, m - 1, h],
+            recv_sem=zs_recv.at[n, way, m - 1, h],
             device_id=zup if way == 0 else zdown,
             device_id_type=MESH,
         )
 
-    def add_and_send(m):
+    def add_and_send(n, m):
+        cols = slice(n * 1024, (n + 1) * 1024)
         for h in (0, 1):
             for way in (0, 1):
                 if h not in hops(way, m):
                     continue
                 sign = 1 if way == 0 else -1
                 if m < 4 and h in hops(way, m + 1):
-                    zsum(way, m + 1, h).wait_recv()
+                    zsum(n, way, m + 1, h).wait_recv()
                     at = slice(32 * AT[sign * m] + 16 * h, 32 * AT[sign * m] + 16 * h + 16)
-                    pz[at] = (
-                        pz[at].astype(F32) + zr[way, m, 16 * h : 16 * h + 16].astype(F32)
+                    pz[at, cols] = (
+                        pz[at, cols].astype(F32) + zr[way, m, 16 * h : 16 * h + 16, cols].astype(F32)
                     ).astype(BF)
-                zsum(way, m, h).start()
-
-    combine(1)
-    add_and_send(4)
-    add_and_send(3)
-    combine(0)
-    add_and_send(2)
-    add_and_send(1)
-
-    for k in (2, 1, 3):
-        share(k).wait_recv()
-    for h in (0, 1):
-        for way in (0, 1):
-            zsum(way, 1, h).wait_recv()
-    for n in range(4):
+                zsum(n, way, m, h).start()
+
+    def last(n):
         cols = slice(n * 1024, (n + 1) * 1024)
+        for h in (0, 1):
+            for way in (0, 1):
+                zsum(n, way, 1, h).wait_recv()
         total = middle[:, cols] + spart[y, :, cols].astype(F32)
-        for k in range(3):
-            total = total + sin[k, :, cols].astype(F32)
+        total = total + snear[0, :, cols].astype(F32) + snear[1, :, cols].astype(F32)
         total = total + pz[0:32, cols].astype(F32)
         total = total + zr[0, 0, :, cols].astype(F32) + zr[1, 0, :, cols].astype(F32)
         out[:, cols] = total.astype(BF)
+
+    for t in range(10):
+        for m in (1, 2, 3):
+            if 0 <= t - 6 + m <= 3:
+                add_and_send(t - 6 + m, m)
+        if 2 <= t < 6:
+            combine(t - 2)
+            add_and_send(t - 2, 4)
+        if 1 <= t < 5:
+            for g in (1, 0):
+                back.relay(g, t - 1)
+        if t < 4:
+            finish_rows(t)
+        if t == 0:
+            downs[3].relay()
+        if t == 2:
+            rows.relay()
+        if t == 4:
+            shared()
+        if t == 6:
+            sums.relay(0)
+        if t == 8:
+            sums.arrived(0)
+            last(0)
+            last(1)
+            last(2)
+    last(3)
 
     for k in range(1, 8):
         tile_copy(k).wait_send()
@@ -723,13 +777,13 @@
         for way in (0, 1):
             for h in hops(way, k):
                 ag(way, k, h).wait_send()
-                zsum(way, k, h).wait_send()
+                for n in range(4):
+                    zsum(n, way, k, h).wait_send()
     for g in (0, 1):
         fwd.sent(g)
-        back.sent(g)
-    for k in (1, 2, 3):
-        rows(k).wait_send()
-        share(k).wait_send()
+        for n in range(4):
+            back.sent(g, n)
+    sums.sent(0)
 
 
 def experts(normed, middle, tile, gate_g, up_g, eg, eu, ed, sg, su, sd):
@@ -763,14 +817,16 @@
             pltpu.VMEM((128, D), BF),
             pltpu.VMEM((4, 32, D), BF),
             pltpu.VMEM((4, 32, D), BF),
-            pltpu.VMEM((3, 32, D), BF),
+            pltpu.VMEM((2, 16, D), BF),
+            pltpu.VMEM((2, 32, D), BF),
             dma((7,)), dma((7,)),
             dma((2, 4, 2)), dma((2, 4, 2)),
-            dma((2, 4, 2)), dma((2, 4, 2)),
-            dma((2, 2, 8)), dma((2, 2, 8)),
-            dma((2, 2, 2)), dma((2, 2, 2)),
-            dma((2, 6)), dma((2, 6)),
-            dma((2, 3)), dma((2, 3)),
+            dma((4, 2, 4, 2)), dma((4, 2, 4, 2)),
+            dma((5, 2, 8)), dma((5, 2, 8)),
+            dma((5, 2, 2)), dma((5, 2, 2)),
+            dma((5, 6)), dma((5, 6)),
+            dma((6,)), dma((6,)),
+            dma((1, 2, 3)), dma((1, 2, 3)),
             dma((15,)),
         ],
         compiler_params=pltpu.CompilerParams(

time: 193 us -> 180 us (0.933)
  Pallas kernels: 187 us -> 176 us
    pallas_call x1, Pallas kernels: 109 us -> 99.1 us  [experts(): pl.pallas_call(experts_kernel, name='experts', out_shape=jax.ShapeDtypeSt...]
where the time goes in v3:
time: 180 us
  Pallas kernels  176 us (98%)
  local copies, waits for them, and re-layouts  3.1 us (2%)
    pallas_call x1, Pallas kernels, experts(): pl.pallas_call(experts_kernel, name='experts', out_shape=jax.ShapeDtypeSt...  99.1 us
    pallas_call x1, Pallas kernels, attend(): pl.pallas_call(attend_kernel, name='attend', out_shape=(jax.ShapeDtypeStr...  77 us

profile of v3, /device:TPU:2, one launch (start us, length us, event | category | flops | bytes accessed | tf_op | source)
XLA Modules:
  0.0 179.9 jit_solution(6492442998601971606)
XLA Ops:
  0.0 0.7 convert_element_type.4
  0.7 0.8 dynamic-slice_bitcast_fusion
  1.5 0.7 tile.10
  2.1 77.0 %attend.1 = (f32[32,4096]{1,0:T(8,128)}, bf16[32,4096]{1,0:T(8,128)(2,1)}, bf16[4,4096,128]{2,1,0:T(8,128)(2,1)}, bf16[4,2048,128]{2,1,0:T(8,128)(2,1)}) custom-call(bf16[128,256]{1,0:T(8,128)(2,1)} %fq.1, bf16[128,128]{1,0:T(8,128)(2,1)} %fk.1, bf16[128,128]{1,0:T(8,128)(2,1)} %fv.1, f32[2,8192]{1,0:T(2,128)} %bitcast.16, bf16[128,256]{1,0:T(8,128)(2,1)} %hq.1, ...), custom_call_target="tpu_custom_call" | custom-call | tf_op jit(solution)/shard_map/attend/pallas_call | solution.py:379
  79.1 99.1 %experts.1 = bf16[32,4096]{1,0:T(8,128)(2,1)} custom-call(bf16[32,4096]{1,0:T(8,128)(2,1)} %get-tuple-element.9.normed, f32[32,4096]{1,0:T(8,128)} %get-tuple-element.10.middle, f32[8,128]{1,0:T(8,128)} %tile.10, bf16[4,4096,128]{2,1,0:T(8,128)(2,1)} %get-tuple-element.11.gate_g, bf16[4,2048,128]{2,1,0:T(8,128)(2,1)} %get-tuple-element.12.up_g, ...), custom_call_target="tpu_custom_call" | custom-call | tf_op jit(solution)/shard_map/experts/pallas_call | solution.py:793
  178.2 1.7 copy.22
  (2 shorter events, 0.0 us)

commit v4 on v3

--- a/solution.py
+++ b/solution.py
@@ -14,6 +14,7 @@
 F32 = jnp.float32
 MESH = pl.DeviceIdType.MESH
 NEG = -1e30
+UP_ROWS = 1024
 
 
 def kv_schedule():
@@ -198,222 +199,6 @@
                 self.copy(n, way, kind).wait_send()
 
 
-def attend_kernel(
-    fq, fk, fv, gf, hq, hk, hv, gh, res, wf, wh, gain, eg, eu,
-    mid_out, norm_out, gate_out, up_out,
-    kva, kvb, qs, acc, mx, tot, att, part, far, near, resv,
-    own_sem, kv_send, kv_recv, w_send, w_recv, rs_send, rs_recv, res_sem,
-):
-    s, y, z, x, c = position()
-    sib = (s + 1 - 2 * c, y)
-    to = {
-        "z+": (sp_of(z + 1, x, c), y),
-        "z-": (sp_of(z - 1, x, c), y),
-        "x+": (sp_of(z, x + 1, c), y),
-        "x-": (sp_of(z, x - 1, c), y),
-    }
-    others = [(s, lax.rem(y + k, 4)) for k in (2, 1, 3)]
-    greet(list(to.values()) + [sib] + others)
-
-    kv = (kva, kvb)
-    pieces = [
-        (fk, kva, 0), (fv, kva, 128), (hk, kvb, 0), (hv, kvb, 128),
-    ]
-    own = [
-        pltpu.make_async_copy(src, dst.at[s, :, pl.ds(at, 128)], own_sem.at[i])
-        for i, (src, dst, at) in enumerate(pieces)
-    ]
-    for copy in own:
-        copy.start()
-    res_copy = pltpu.make_async_copy(res.at[pl.ds(y * 32, 32)], resv, res_sem)
-    res_copy.start()
-
-    def hop(prt, idx, device):
-        return pltpu.make_async_remote_copy(
-            src_ref=kv[prt].at[idx],
-            dst_ref=kv[prt].at[idx],
-            send_sem=kv_send.at[prt],
-            recv_sem=kv_recv.at[prt, idx],
-            device_id=device,
-            device_id_type=MESH,
-        )
-
-    own_events, events = kv_schedule()
-    for prt, _, _, links in own_events:
-        own[2 * prt].wait()
-        own[2 * prt + 1].wait()
-        for link in links:
-            hop(prt, s, to[link]).start()
-        hop(prt, s, sib).start()
-
-    half_rows = 2048
-    gates = YGather(
-        [eg.at[pl.ds(h * half_rows, half_rows)] for h in (0, 1)],
-        lambda j, h: gate_out.at[j, pl.ds(h * half_rows, half_rows)],
-        w_send.at[0], w_recv.at[0],
-    )
-    ups = YGather(
-        [eu.at[pl.ds(h * 1024, 1024)] for h in (0, 1)],
-        lambda j, h: up_out.at[j, pl.ds(h * 1024, 1024)],
-        w_send.at[1], w_recv.at[1],
-    )
-    gates.start()
-    ups.start()
-
-    lane = lax.broadcasted_iota(jnp.int32, (128, 128), 1)
-    qs[0, 0:128] = fq[:, 0:128]
-    qs[0, 128:256] = fq[:, 128:256]
-    h01 = hq[:, 0:128].astype(F32)
-    h23 = hq[:, 128:256].astype(F32)
-    qs[1, 0:128] = jnp.where(lane < 64, h01, 0.0).astype(BF)
-    qs[1, 128:256] = jnp.where(lane < 64, pltpu.roll(h01, 64, 1), 0.0).astype(BF)
-    qs[2, 0:128] = jnp.where(lane >= 64, pltpu.roll(h23, 64, 1), 0.0).astype(BF)
-    qs[2, 128:256] = jnp.where(lane >= 64, h23, 0.0).astype(BF)
-    acc[...] = jnp.zeros_like(acc)
-    tot[...] = jnp.zeros_like(tot)
-    mx[...] = jnp.full_like(mx, NEG)
-
-    for i, (prt, dz, dx, links) in enumerate(events):
-        idx = sp_of(z - dz, x - dx, c)
-        hop(prt, idx, sib).wait_recv()
-        for link in links:
-            hop(prt, idx, to[link]).start()
-        hop(prt, idx, sib).start()
-        if i == 30:
-            gates.relay()
-    ups.relay()
-
-    @pl.loop(0, 32)
-    def _(i):
-        idx = 2 * i + 1 - c
-        for prt in (0, 1):
-            hop(prt, idx, sib).wait_recv()
-
-    row0 = s * 128
-    gfirst = gf[:, pl.ds(pl.multiple_of(row0, 128), 128)][:, 0:1]
-    hfirst = gh[:, pl.ds(pl.multiple_of(row0, 128), 128)][:, 0:1]
-
-    def chunk(at, masked):
-        key0 = pl.multiple_of(at * 1024, 1024)
-        fg = (gf[:, pl.ds(key0, 1024)] - gfirst) * LOG2E
-        hg = (gh[:, pl.ds(key0, 1024)] - hfirst) * LOG2E
-        if masked:
-            qpos = (s % 8) * 128 + lax.broadcasted_iota(jnp.int32, (128, 1024), 0)
-            kpos = lax.broadcasted_iota(jnp.int32, (128, 1024), 1)
-            allowed = kpos <= qpos
-        for g in range(3):
-            store = kva if g == 0 else kvb
-            k = store[pl.ds(at * 8, 8), :, 0:128].reshape(1024, 128)
-            v = store[pl.ds(at * 8, 8), :, 128:256].reshape(1024, 128)
-            scale = (128 ** -0.5 if g == 0 else 0.125) * LOG2E
-            scores = lax.dot_general(
-                qs[g], k, (((1,), (1,)), ((), ())), preferred_element_type=F32
-            )
-            for r in (0, 1):
-                row = fg[r : r + 1] if g == 0 else hg[2 * (g - 1) + r : 2 * (g - 1) + r + 1]
-                t = scores[r * 128 : (r + 1) * 128] * scale - row
-                if masked:
-                    t = jnp.where(allowed, t, NEG)
-                old = mx[g, pl.ds(r * 128, 128)]
-                new = jnp.maximum(old, jnp.max(t, axis=1, keepdims=True))
-                p = jnp.exp2(t - new[:, 0:1])
-                shrink = jnp.exp2(old - new)
-                mx[g, pl.ds(r * 128, 128)] = new
-                tot[g, pl.ds(r * 128, 128)] = (
-                    tot[g, pl.ds(r * 128, 128)] * shrink + jnp.sum(p, axis=1, keepdims=True)
-                )
-                acc[g, pl.ds(r * 128, 128)] = acc[g, pl.ds(r * 128, 128)] * shrink + jnp.dot(
-                    p.astype(BF), v, preferred_element_type=F32
-                )
-
-    @pl.loop(0, z)
-    def _(at):
-        chunk(at, False)
-
-    chunk(z, True)
-
-    outs = [
-        [acc[g, r * 128 : (r + 1) * 128] / tot[g, r * 128 : (r + 1) * 128] for r in (0, 1)]
-        for g in range(3)
-    ]
-    att[:, 0:128] = outs[0][0].astype(BF)
-    att[:, 128:256] = outs[0][1].astype(BF)
-    att[:, 256:384] = jnp.where(lane < 64, outs[1][0], pltpu.roll(outs[1][1], 64, 1)).astype(BF)
-    att[:, 384:512] = jnp.where(lane < 64, pltpu.roll(outs[2][0], 64, 1), outs[2][1]).astype(BF)
-
-    gates.finish()
-    ups.finish()
-
-    sums = YReduce(part, far, near, rs_send, rs_recv, 1024)
-    for n in range(4):
-        cols = slice(n * 1024, (n + 1) * 1024)
-        product = jnp.dot(att[:, 0:256], wf[:, cols], preferred_element_type=F32) + jnp.dot(
-            att[:, 256:512], wh[:, cols], preferred_element_type=F32
-        )
-        part[:, :, cols] = product.astype(BF).reshape(4, 32, 1024)
-        sums.start(n)
-    for n in range(4):
-        sums.relay(n)
-    res_copy.wait()
-    square = jnp.zeros((32, 1), F32)
-    for n in range(4):
-        cols = slice(n * 1024, (n + 1) * 1024)
-        total = resv[:, cols].astype(F32) + part[y, :, cols].astype(F32)
-        sums.arrived(n)
-        total = total + near[0, :, cols].astype(F32) + near[1, :, cols].astype(F32)
-        mid_out[:, cols] = total
-        square = square + jnp.sum(total * total, axis=1, keepdims=True)
-    factor = lax.rsqrt(square * (1.0 / D) + 1e-06)
-    norm_out[...] = (mid_out[...] * factor * gain[...]).astype(BF)
-
-    for n in range(4):
-        sums.sent(n)
-    for prt in (0, 1):
-        everything = kv[prt].at[pl.ds(0, 63)]
-        pltpu.make_async_copy(everything, everything, kv_send.at[prt]).wait()
-
-
-def attend(fq, fk, fv, gf, hq, hk, hv, gh, res, wf, wh, gain, eg, eu):
-    vmem = pl.BlockSpec(memory_space=pltpu.VMEM)
-    anym = pl.BlockSpec(memory_space=pl.ANY)
-    return pl.pallas_call(
-        attend_kernel,
-        name="attend",
-        out_shape=(
-            jax.ShapeDtypeStruct((32, D), F32),
-            jax.ShapeDtypeStruct((32, D), BF),
-            jax.ShapeDtypeStruct((4, 4096, 128), BF),
-            jax.ShapeDtypeStruct((4, 2048, 128), BF),
-        ),
-        in_specs=[vmem, anym, anym, vmem, vmem, anym, anym, vmem, anym, vmem, vmem, vmem, anym, anym],
-        out_specs=[vmem, vmem, anym, anym],
-        scratch_shapes=[
-            pltpu.VMEM((64, 128, 256), BF),
-            pltpu.VMEM((64, 128, 256), BF),
-            pltpu.VMEM((3, 256, 128), BF),
-            pltpu.VMEM((3, 256, 128), F32),
-            pltpu.VMEM((3, 256, 128), F32),
-            pltpu.VMEM((3, 256, 128), F32),
-            pltpu.VMEM((128, 512), BF),
-            pltpu.VMEM((4, 32, D), BF),
-            pltpu.VMEM((2, 16, D), BF),
-            pltpu.VMEM((2, 32, D), BF),
-            pltpu.VMEM((32, D), BF),
-            pltpu.SemaphoreType.DMA((4,)),
-            pltpu.SemaphoreType.DMA((2,)),
-            pltpu.SemaphoreType.DMA((2, 64)),
-            pltpu.SemaphoreType.DMA((2, 6)),
-            pltpu.SemaphoreType.DMA((2, 6)),
-            pltpu.SemaphoreType.DMA((4, 2, 3)),
-            pltpu.SemaphoreType.DMA((4, 2, 3)),
-            pltpu.SemaphoreType.DMA,
-        ],
-        compiler_params=pltpu.CompilerParams(
-            collective_id=0, has_side_effects=True, vmem_limit_bytes=56 * 1024 * 1024
-        ),
-    )(fq, fk, fv, gf, hq, hk, hv, gh, res, wf, wh, gain, eg, eu)
-
-
 REL = (0, -1, 1, -2, 2, -3, 3, 4)
 AT = {r: i for i, r in enumerate(REL)}
 AT[-4] = AT[4]
@@ -494,42 +279,72 @@
             self.passed(g, crel, n).wait_send()
 
 
-def experts_kernel(
-    normed, middle, tile, gate_g, up_g, eg, eu, ed, sg, su, sd,
+def layer_kernel(
+    fq, fk, fv, gf, hq, hk, hv, gh, res, wf, wh, gain, tile, eg, eu, ed, sg, su, sd,
     out,
-    tiles, tok, sel, wts, sb, xr, yb, yr, rl0, rl1, pz, zr, gu, dn, hid, sgv, suv, sdv, nall, spart, sfar, snear,
+    kva, kvb, qs, acc, mx, tot, att, part, far, near, resv, mid, wfv, whv,
+    tiles, tok, sel, wts, sb, xr, yb, yr, rl0, rl1, pz, zr, gu, dn, hid, sgv, suv, sdv, nall, spart,
+    sfar, snear,
+    own_sem, kv_send, kv_recv, rs_send, rs_recv, res_sem,
     tile_send, tile_recv, ag_send, ag_recv, zs_send, zs_recv,
     x_send, x_recv, xr_send, xr_recv, w_send, w_recv, g_send, g_recv, s_send, s_recv, ld,
 ):
     s, y, z, x, c = position()
-    zup, zdown = (sp_of(z + 1, x, c), y), (sp_of(z - 1, x, c), y)
+    sib = (s + 1 - 2 * c, y)
+    to = {
+        "z+": (sp_of(z + 1, x, c), y),
+        "z-": (sp_of(z - 1, x, c), y),
+        "x+": (sp_of(z, x + 1, c), y),
+        "x-": (sp_of(z, x - 1, c), y),
+    }
+    zup, zdown = to["z+"], to["z-"]
     zs = [(sp_of(z + k, x, c), y) for k in range(1, 8)]
     xs = [(sp_of(z, x + d, core), y) for d in (1, 3) for core in (c, 1 - c)]
-    sib = (s + 1 - 2 * c, y)
-    others = [(s, lax.rem(y + k, 4)) for k in (1, 2, 3)]
-    greet(zs + xs + [sib] + others)
+    greet(zs + xs + [sib] + [(s, lax.rem(y + k, 4)) for k in (1, 2, 3)])
+
+    kv = (kva, kvb)
+    pieces = [
+        (fk, kva, 0), (fv, kva, 128), (hk, kvb, 0), (hv, kvb, 128),
+    ]
+    own = [
+        pltpu.make_async_copy(src, dst.at[s, :, pl.ds(at, 128)], own_sem.at[i])
+        for i, (src, dst, at) in enumerate(pieces)
+    ]
+    for copy in own:
+        copy.start()
+    res_copy = pltpu.make_async_copy(res.at[pl.ds(y * 32, 32)], resv, res_sem)
+    res_copy.start()
 
     loads = [
         pltpu.make_async_copy(tile, tiles.at[z], ld.at[0]),
-        pltpu.make_async_copy(normed, tok.at[pl.ds(0, 32)], ld.at[1]),
-        pltpu.make_async_copy(normed, nall.at[y], ld.at[2]),
-        pltpu.make_async_copy(eg, gu.at[y, :, pl.ds(0, 128)], ld.at[3]),
-        pltpu.make_async_copy(eu, gu.at[y, :, pl.ds(128, 128)], ld.at[4]),
-        pltpu.make_async_copy(ed, dn.at[pl.ds(y * 128, 128)], ld.at[5]),
-        pltpu.make_async_copy(sg, sgv, ld.at[6]),
-        pltpu.make_async_copy(su, suv, ld.at[7]),
-        pltpu.make_async_copy(sd, sdv, ld.at[8]),
+        pltpu.make_async_copy(eg, gu.at[y, :, pl.ds(0, 128)], ld.at[1]),
+        pltpu.make_async_copy(eu, gu.at[y, :, pl.ds(128, 128)], ld.at[2]),
+        pltpu.make_async_copy(ed, dn.at[pl.ds(y * 128, 128)], ld.at[3]),
+        pltpu.make_async_copy(sg, sgv, ld.at[4]),
+        pltpu.make_async_copy(su, suv, ld.at[5]),
+        pltpu.make_async_copy(sd, sdv, ld.at[6]),
+        pltpu.make_async_copy(wf, wfv, ld.at[7]),
+        pltpu.make_async_copy(wh, whv, ld.at[8]),
     ]
-    for k in (1, 2, 3):
-        j = lax.rem(y + k, 4)
-        loads.append(pltpu.make_async_copy(gate_g.at[j], gu.at[j, :, pl.ds(0, 128)], ld.at[7 + 2 * k]))
-        loads.append(
-            pltpu.make_async_copy(up_g.at[j], gu.at[j, pl.ds(0, 2048), pl.ds(128, 128)], ld.at[8 + 2 * k])
-        )
-    for copy in loads:
-        copy.start()
-
-    loads[0].wait()
+    loads[0].start()
+
+    def hop(prt, idx, device):
+        return pltpu.make_async_remote_copy(
+            src_ref=kv[prt].at[idx],
+            dst_ref=kv[prt].at[idx],
+            send_sem=kv_send.at[prt],
+            recv_sem=kv_recv.at[prt, idx],
+            device_id=device,
+            device_id_type=MESH,
+        )
+
+    own_events, events = kv_schedule()
+    for prt, _, _, links in own_events:
+        own[2 * prt].wait()
+        own[2 * prt + 1].wait()
+        for link in links:
+            hop(prt, s, to[link]).start()
+        hop(prt, s, sib).start()
 
     def tile_copy(k):
         return pltpu.make_async_remote_copy(
@@ -541,55 +356,141 @@
             device_id_type=MESH,
         )
 
+
+    loads[0].wait()
     for k in range(1, 8):
         tile_copy(k).start()
 
-    def ag(way, k, h):
-        sign = -1 if way == 0 else 1
-        return pltpu.make_async_remote_copy(
-            src_ref=tok.at[pl.ds(32 * AT[sign * (k - 1)] + 16 * h, 16)],
-            dst_ref=tok.at[pl.ds(32 * AT[sign * k] + 16 * h, 16)],
-            send_sem=ag_send.at[way, k - 1, h],
-            recv_sem=ag_recv.at[way, k - 1, h],
-            device_id=zup if way == 0 else zdown,
-            device_id_type=MESH,
-        )
-
-    def hops(way, k):
-        return (0, 1) if k < 4 else ((0,) if way == 0 else (1,))
-
-    loads[1].wait()
-    for h in (0, 1):
-        for way in (0, 1):
-            ag(way, 1, h).start()
-
-    ups = YGather(
-        [eu.at[pl.ds(2048 + h * 1024, 1024)] for h in (0, 1)],
-        lambda j, h: gu.at[j, pl.ds(2048 + h * 1024, 1024), pl.ds(128, 128)],
+    gates = YGather(
+        [eg.at[pl.ds(h * 2048, 2048)] for h in (0, 1)],
+        lambda j, h: gu.at[j, pl.ds(h * 2048, 2048), pl.ds(0, 128)],
         w_send.at[0], w_recv.at[0],
     )
-    def down_chunk(n):
-        cols = pl.ds(n * 1024, 1024)
+
+    def up_rows(at, count, slot):
         return YGather(
-            [ed.at[pl.ds(h * 64, 64), cols] for h in (0, 1)],
-            lambda j, h: dn.at[pl.ds(j * 128 + h * 64, 64), cols],
-            w_send.at[1 + n], w_recv.at[1 + n],
-        )
-
-    downs = [down_chunk(n) for n in range(4)]
-    rows = YGather(
-        [normed.at[pl.ds(h * 16, 16)] for h in (0, 1)],
-        lambda j, h: nall.at[j, pl.ds(h * 16, 16)],
-        g_send, g_recv,
-    )
-    ups.start()
-    downs[0].start()
-    downs[1].start()
-
+            [eu.at[pl.ds(at + h * count // 2, count // 2)] for h in (0, 1)],
+            lambda j, h: gu.at[j, pl.ds(at + h * count // 2, count // 2), pl.ds(128, 128)],
+            w_send.at[slot], w_recv.at[slot],
+        )
+
+    ups0 = up_rows(0, UP_ROWS, 1)
+    ups = up_rows(UP_ROWS, 4096 - UP_ROWS, 2)
+    gates.start()
+    ups0.start()
+    for copy in loads[1:]:
+        copy.start()
+
+    lane = lax.broadcasted_iota(jnp.int32, (128, 128), 1)
+    qs[0, 0:128] = fq[:, 0:128]
+    qs[0, 128:256] = fq[:, 128:256]
+    h01 = hq[:, 0:128].astype(F32)
+    h23 = hq[:, 128:256].astype(F32)
+    qs[1, 0:128] = jnp.where(lane < 64, h01, 0.0).astype(BF)
+    qs[1, 128:256] = jnp.where(lane < 64, pltpu.roll(h01, 64, 1), 0.0).astype(BF)
+    qs[2, 0:128] = jnp.where(lane >= 64, pltpu.roll(h23, 64, 1), 0.0).astype(BF)
+    qs[2, 128:256] = jnp.where(lane >= 64, h23, 0.0).astype(BF)
+    acc[...] = jnp.zeros_like(acc)
+    tot[...] = jnp.zeros_like(tot)
+    mx[...] = jnp.full_like(mx, NEG)
+
+    row0 = s * 128
+    gfirst = gf[:, pl.ds(pl.multiple_of(row0, 128), 128)][:, 0:1]
+    hfirst = gh[:, pl.ds(pl.multiple_of(row0, 128), 128)][:, 0:1]
+
+    def attend_to(plane, g, masked):
+        key0 = pl.multiple_of(plane * 1024, 1024)
+        if g == 0:
+            gate = (gf[:, pl.ds(key0, 1024)] - gfirst) * LOG2E
+        else:
+            gate = (gh[:, pl.ds(key0, 1024)] - hfirst) * LOG2E
+        store = kva if g == 0 else kvb
+        k = store[pl.ds(plane * 8, 8), :, 0:128].reshape(1024, 128)
+        v = store[pl.ds(plane * 8, 8), :, 128:256].reshape(1024, 128)
+        scale = (128 ** -0.5 if g == 0 else 0.125) * LOG2E
+        scores = lax.dot_general(
+            qs[g], k, (((1,), (1,)), ((), ())), preferred_element_type=F32
+        )
+        for r in (0, 1):
+            head = r if g == 0 else 2 * (g - 1) + r
+            t = scores[r * 128 : (r + 1) * 128] * scale - gate[head : head + 1]
+            if masked:
+                qpos = (s % 8) * 128 + lax.broadcasted_iota(jnp.int32, (128, 1024), 0)
+                kpos = lax.broadcasted_iota(jnp.int32, (128, 1024), 1)
+                t = jnp.where(kpos <= qpos, t, NEG)
+            old = mx[g, pl.ds(r * 128, 128)]
+            new = jnp.maximum(old, jnp.max(t, axis=1, keepdims=True))
+            p = jnp.exp2(t - new[:, 0:1])
+            shrink = jnp.exp2(old - new)
+            mx[g, pl.ds(r * 128, 128)] = new
+            tot[g, pl.ds(r * 128, 128)] = (
+                tot[g, pl.ds(r * 128, 128)] * shrink + jnp.sum(p, axis=1, keepdims=True)
+            )
+            acc[g, pl.ds(r * 128, 128)] = acc[g, pl.ds(r * 128, 128)] * shrink + jnp.dot(
+                p.astype(BF), v, preferred_element_type=F32
+            )
+
+    waiting = []
+    for dz in range(-3, 5):
+        for g in range(3):
+            last = max(
+                i for i, (prt, edz, *_) in enumerate(events) if edz == dz and prt == min(g, 1)
+            )
+            waiting.append((last + 3, g, dz))
+    waiting.sort()
+
+    def next_item():
+        _, g, dz = waiting.pop(0)
+        plane = lax.rem(z - dz + 8, 8)
+        if g < 2:
+            for col in range(4):
+                hop(g, sp_of(plane, col, 1 - c), sib).wait_recv()
+        if dz == 0:
+            attend_to(z, g, True)
+        else:
+
+            @pl.when(plane < z)
+            def _():
+                attend_to(plane, g, False)
+
+    for i, (prt, dz, dx, links) in enumerate(events):
+        idx = sp_of(z - dz, x - dx, c)
+        hop(prt, idx, sib).wait_recv()
+        for link in links:
+            hop(prt, idx, to[link]).start()
+        hop(prt, idx, sib).start()
+        if waiting and waiting[0][0] <= i:
+            next_item()
+        if i == 30:
+            gates.relay()
+        if i == 46:
+            ups0.relay()
+    while waiting:
+        next_item()
+
+    outs = [
+        [acc[g, r * 128 : (r + 1) * 128] / tot[g, r * 128 : (r + 1) * 128] for r in (0, 1)]
+        for g in range(3)
+    ]
+    att[:, 0:128] = outs[0][0].astype(BF)
+    att[:, 128:256] = outs[0][1].astype(BF)
+    att[:, 256:384] = jnp.where(lane < 64, outs[1][0], pltpu.roll(outs[1][1], 64, 1)).astype(BF)
+    att[:, 384:512] = jnp.where(lane < 64, pltpu.roll(outs[2][0], 64, 1), outs[2][1]).astype(BF)
+
+    for copy in loads[7:]:
+        copy.wait()
+    asums = YReduce(part, far, near, rs_send, rs_recv, 1024)
+    for n in range(4):
+        cols = slice(n * 1024, (n + 1) * 1024)
+        product = jnp.dot(att[:, 0:256], wfv[:, cols], preferred_element_type=F32) + jnp.dot(
+            att[:, 256:512], whv[:, cols], preferred_element_type=F32
+        )
+        part[:, :, cols] = product.astype(BF).reshape(4, 32, 1024)
+        asums.start(n)
     for k in range(1, 8):
         tile_copy(k).wait_recv()
 
-    lane = lax.broadcasted_iota(jnp.int32, (4, 128), 1) // 32
+    lane4 = lax.broadcasted_iota(jnp.int32, (4, 128), 1) // 32
     row16 = lax.broadcasted_iota(jnp.int32, (16, 128), 0)
     lane16 = lax.broadcasted_iota(jnp.int32, (16, 128), 1) // 32
     r0 = lax.broadcasted_iota(jnp.int32, (128, 128), 0)
@@ -601,8 +502,8 @@
         scale = jnp.zeros((4, 128), F32)
         for i in range(4):
             src = lax.rem(z + REL[g * 4 + i] + 8, 8)
-            names = jnp.where(lane == i, tiles[src, 0:4], names)
-            scale = jnp.where(lane == i, tiles[src, 4:8], scale)
+            names = jnp.where(lane4 == i, tiles[src, 0:4], names)
+            scale = jnp.where(lane4 == i, tiles[src, 4:8], scale)
         occ, wrow = [], []
         for d in range(4):
             for crel in (0, 1):
@@ -627,6 +528,61 @@
         wts[g, 0] = high
         wts[g, 1] = (full - high.astype(F32)).astype(BF)
 
+    picks(0)
+    picks(1)
+    for n in range(4):
+        asums.relay(n)
+    ups.start()
+    res_copy.wait()
+    square = jnp.zeros((32, 1), F32)
+    for n in range(4):
+        cols = slice(n * 1024, (n + 1) * 1024)
+        total = resv[:, cols].astype(F32) + part[y, :, cols].astype(F32)
+        asums.arrived(n)
+        total = total + near[0, :, cols].astype(F32) + near[1, :, cols].astype(F32)
+        mid[:, cols] = total
+        square = square + jnp.sum(total * total, axis=1, keepdims=True)
+    factor = lax.rsqrt(square * (1.0 / D) + 1e-06)
+    for n in range(4):
+        cols = slice(n * 1024, (n + 1) * 1024)
+        normed = (mid[:, cols] * factor * gain[:, cols]).astype(BF)
+        tok[0:32, cols] = normed
+        nall[y, :, cols] = normed
+
+    def ag(way, k, h):
+        sign = -1 if way == 0 else 1
+        return pltpu.make_async_remote_copy(
+            src_ref=tok.at[pl.ds(32 * AT[sign * (k - 1)] + 16 * h, 16)],
+            dst_ref=tok.at[pl.ds(32 * AT[sign * k] + 16 * h, 16)],
+            send_sem=ag_send.at[way, k - 1, h],
+            recv_sem=ag_recv.at[way, k - 1, h],
+            device_id=zup if way == 0 else zdown,
+            device_id_type=MESH,
+        )
+
+    def hops(way, k):
+        return (0, 1) if k < 4 else ((0,) if way == 0 else (1,))
+
+    for h in (0, 1):
+        for way in (0, 1):
+            ag(way, 1, h).start()
+
+    def down_chunk(n):
+        cols = pl.ds(n * 1024, 1024)
+        return YGather(
+            [ed.at[pl.ds(h * 64, 64), cols] for h in (0, 1)],
+            lambda j, h: dn.at[pl.ds(j * 128 + h * 64, 64), cols],
+            w_send.at[3 + n], w_recv.at[3 + n],
+        )
+
+    downs = [down_chunk(n) for n in range(4)]
+    rows = YGather(
+        [nall.at[y, pl.ds(h * 16, 16)] for h in (0, 1)],
+        lambda j, h: nall.at[j, pl.ds(h * 16, 16)],
+        g_send, g_recv,
+    )
+    downs[0].start()
+
     fwd = Exchange(sb, xr, rl0, x_send.at[pl.ds(0, 1)], x_recv.at[pl.ds(0, 1)], xr_send.at[pl.ds(0, 1)], xr_recv.at[pl.ds(0, 1)], D)
     back = Exchange(yb, yr, rl1, x_send.at[pl.ds(1, 4)], x_recv.at[pl.ds(1, 4)], xr_send.at[pl.ds(1, 4)], xr_recv.at[pl.ds(1, 4)], 1024)
 
@@ -638,8 +594,6 @@
             ).astype(BF)
         fwd.start(g)
 
-    picks(0)
-    picks(1)
     for k in range(1, 5):
         for h in (0, 1):
             for way in (0, 1):
@@ -650,19 +604,22 @@
         if k == 2:
             select(0)
             ups.relay()
-            downs[2].start()
-            downs[3].start()
+            downs[1].start()
         if k == 3:
             fwd.relay(0)
             downs[0].relay()
+            downs[2].start()
     select(1)
     downs[1].relay()
+    downs[3].start()
 
     fwd.relay(1)
     downs[2].relay()
     rows.start()
-    for copy in loads[2:]:
+    for copy in loads[1:7]:
         copy.wait()
+    gates.finish()
+    ups0.finish()
     ups.finish()
     fwd.arrived(0)
     fwd.arrived(1)
@@ -738,7 +695,7 @@
         for h in (0, 1):
             for way in (0, 1):
                 zsum(n, way, 1, h).wait_recv()
-        total = middle[:, cols] + spart[y, :, cols].astype(F32)
+        total = mid[:, cols] + spart[y, :, cols].astype(F32)
         total = total + snear[0, :, cols].astype(F32) + snear[1, :, cols].astype(F32)
         total = total + pz[0:32, cols].astype(F32)
         total = total + zr[0, 0, :, cols].astype(F32) + zr[1, 0, :, cols].astype(F32)
@@ -785,54 +742,45 @@
             back.sent(g, n)
     sums.sent(0)
 
-
-def experts(normed, middle, tile, gate_g, up_g, eg, eu, ed, sg, su, sd):
+    for n in range(4):
+        asums.sent(n)
+    for prt in (0, 1):
+        everything = kv[prt].at[pl.ds(0, 63)]
+        pltpu.make_async_copy(everything, everything, kv_send.at[prt]).wait()
+
+
+def layer(*args):
     vmem = pl.BlockSpec(memory_space=pltpu.VMEM)
     anym = pl.BlockSpec(memory_space=pl.ANY)
     dma = pltpu.SemaphoreType.DMA
+    bf = lambda *shape: pltpu.VMEM(shape, BF)
     return pl.pallas_call(
-        experts_kernel,
-        name="experts",
+        layer_kernel,
+        name="layer",
         out_shape=jax.ShapeDtypeStruct((32, D), BF),
-        in_specs=[anym, vmem] + [anym] * 9,
+        in_specs=[vmem, anym, anym, vmem, vmem, anym, anym, vmem, anym, anym, anym, vmem] + [anym] * 7,
         out_specs=vmem,
         scratch_shapes=[
-            pltpu.VMEM((8, 8, 128), F32),
-            pltpu.VMEM((256, D), BF),
-            pltpu.VMEM((2, 128, 128), BF),
-            pltpu.VMEM((2, 2, 128, 128), BF),
-            pltpu.VMEM((256, D), BF),
-            pltpu.VMEM((256, D), BF),
-            pltpu.VMEM((256, D), BF),
-            pltpu.VMEM((256, D), BF),
-            pltpu.VMEM((2, 2, 16, D), BF),
-            pltpu.VMEM((2, 2, 16, D), BF),
-            pltpu.VMEM((256, D), BF),
-            pltpu.VMEM((2, 4, 32, D), BF),
-            pltpu.VMEM((4, 4096, 256), BF),
-            pltpu.VMEM((512, D), BF),
-            pltpu.VMEM((256, 512), BF),
-            pltpu.VMEM((4096, 128), BF),
-            pltpu.VMEM((4096, 128), BF),
-            pltpu.VMEM((128, D), BF),
-            pltpu.VMEM((4, 32, D), BF),
-            pltpu.VMEM((4, 32, D), BF),
-            pltpu.VMEM((2, 16, D), BF),
-            pltpu.VMEM((2, 32, D), BF),
-            dma((7,)), dma((7,)),
-            dma((2, 4, 2)), dma((2, 4, 2)),
-            dma((4, 2, 4, 2)), dma((4, 2, 4, 2)),
-            dma((5, 2, 8)), dma((5, 2, 8)),
-            dma((5, 2, 2)), dma((5, 2, 2)),
-            dma((5, 6)), dma((5, 6)),
-            dma((6,)), dma((6,)),
-            dma((1, 2, 3)), dma((1, 2, 3)),
-            dma((15,)),
+            bf(64, 128, 256), bf(64, 128, 256), bf(3, 256, 128),
+            pltpu.VMEM((3, 256, 128), F32), pltpu.VMEM((3, 256, 128), F32),
+            pltpu.VMEM((3, 256, 128), F32),
+            bf(128, 512), bf(4, 32, D), bf(2, 16, D), bf(2, 32, D), bf(32, D),
+            pltpu.VMEM((32, D), F32), bf(256, D), bf(256, D),
+            pltpu.VMEM((8, 8, 128), F32), bf(256, D), bf(2, 128, 128), bf(2, 2, 128, 128),
+            bf(256, D), bf(256, D), bf(256, D), bf(256, D), bf(2, 2, 16, D), bf(2, 2, 16, D),
+            bf(256, D), bf(2, 4, 32, D), bf(4, 4096, 256), bf(512, D), bf(256, 512),
+            bf(4096, 128), bf(4096, 128), bf(128, D), bf(4, 32, D), bf(4, 32, D),
+            bf(2, 16, D), bf(2, 32, D),
+            dma((4,)), dma((2,)), dma((2, 64)), dma((4, 2, 3)), dma((4, 2, 3)), dma,
+            dma((7,)), dma((7,)), dma((2, 4, 2)), dma((2, 4, 2)),
+            dma((4, 2, 4, 2)), dma((4, 2, 4, 2)), dma((5, 2, 8)), dma((5, 2, 8)),
+            dma((5, 2, 2)), dma((5, 2, 2)), dma((7, 6)), dma((7, 6)), dma((6,)), dma((6,)),
+            dma((1, 2, 3)), dma((1, 2, 3)), dma((9,)),
         ],
         compiler_params=pltpu.CompilerParams(
-            collective_id=1, has_side_effects=True, vmem_limit_bytes=60 * 1024 * 1024
+            collective_id=0, has_side_effects=True, vmem_limit_bytes=62 * 1024 * 1024
         ),
-    )(normed, middle, tile, gate_g, up_g, eg, eu, ed, sg, su, sd)
+    )(*args)
 
 
 def body(
@@ -843,14 +791,10 @@
     quarter = lax.axis_index("tp")
     own = lambda a: lax.dynamic_slice_in_dim(a.T.astype(F32), quarter * 32, 32, 1)
     tile = jnp.tile(jnp.concatenate([own(routes), own(route_weights)], axis=0), (1, 4))
-    middle, normed, gates, ups = attend(
+    return layer(
         full_queries, full_keys, full_values, full_gates.T, half_queries, half_keys, half_values,
-        half_gates.T, residual, full_output, half_output, norm_gain.reshape(1, D),
-        expert_gate[0], expert_up[0],
-    )
-    return experts(
-        normed, middle, tile, gates, ups, expert_gate[0], expert_up[0], expert_down[0],
-        shared_gate, shared_up, shared_down,
+        half_gates.T, residual, full_output, half_output, norm_gain.reshape(1, D), tile,
+        expert_gate[0], expert_up[0], expert_down[0], shared_gate, shared_up, shared_down,
     )
 
 

time: 180 us -> 167 us (0.928)
  Pallas kernels: 176 us -> 163 us
    pallas_call x2 -> x1, Pallas kernels: 176 us -> 163 us  [layer(): pl.pallas_call(layer_kernel, name='layer', out_shape=jax.ShapeDtypeStruct...]
where the time goes in v4:
time: 167 us
  Pallas kernels  163 us (98%)
  local copies, waits for them, and re-layouts  3.1 us (2%)
    pallas_call x1, Pallas kernels, layer(): pl.pallas_call(layer_kernel, name='layer', out_shape=jax.ShapeDtypeStruct...  163 us

profile of v4, /device:TPU:2, one launch (start us, length us, event | category | flops | bytes accessed | tf_op | source)
XLA Modules:
  0.0 166.9 jit_solution(13913085019878218107)
XLA Ops:
  0.0 0.7 convert_element_type.4
  0.7 0.8 dynamic-slice_bitcast_fusion
  1.5 0.7 tile.10
  2.1 163.1 %layer.1 = bf16[32,4096]{1,0:T(8,128)(2,1)} custom-call(bf16[128,256]{1,0:T(8,128)(2,1)} %fq.1, bf16[128,128]{1,0:T(8,128)(2,1)} %fk.1, bf16[128,128]{1,0:T(8,128)(2,1)} %fv.1, f32[2,8192]{1,0:T(2,128)} %bitcast.14, bf16[128,256]{1,0:T(8,128)(2,1)} %hq.1, bf16[128,128]{1,0:T(8,128)(2,1)} %hk.1, bf16[128,128]{1,0:T(8,128)(2,1)} %hv.1, f32[4,8192]{1,0:T(4,128)} %bitcast.13, ...), custom_call_target="tpu_custom_call" | custom-call | tf_op jit(solution)/shard_map/layer/pallas_call | solution.py:757
  165.2 1.7 %copy.22 = bf16[32,4096]{1,0:T(8,128)(2,1)} copy(bf16[32,4096]{1,0:T(8,128)(2,1)} %layer.1) | data formatting | bytes 524288
  (2 shorter events, 0.0 us)

commit v5 on v4

--- a/solution.py
+++ b/solution.py
@@ -59,10 +59,10 @@
             ndz = 4
         if link[0] == "x" and ndx == -2:
             ndx = 2
-        heapq.heappush(heap, (free[link] + 1.5, count, part, ndz, ndx, link))
+        heapq.heappush(heap, (free[link] + 2.5, count, part, ndz, ndx, link))
         count += 1
 
-    for part in (1, 0):
+    for part in (0, 1):
         for link in onward(part, 0, 0, "own"):
             send(0.0, part, 0, 0, link)
     seen = set()
@@ -75,7 +75,7 @@
         for out in links:
             send(now, part, dz, dx, out)
     assert len(events) == 62
-    own = [(part, 0, 0, tuple(onward(part, 0, 0, "own"))) for part in (1, 0)]
+    own = [(part, 0, 0, tuple(onward(part, 0, 0, "own"))) for part in (0, 1)]
     return own, events
 
 
@@ -280,7 +280,7 @@
 
 
 def layer_kernel(
-    fq, fk, fv, gf, hq, hk, hv, gh, res, wf, wh, gain, tile, eg, eu, ed, sg, su, sd,
+    fq, fk, fv, gf, hq, hk, hv, gh, res, wf, wh, gain, names_in, scale_in, eg, eu, ed, sg, su, sd,
     out,
     kva, kvb, qs, acc, mx, tot, att, part, far, near, resv, mid, wfv, whv,
     tiles, tok, sel, wts, sb, xr, yb, yr, rl0, rl1, pz, zr, gu, dn, hid, sgv, suv, sdv, nall, spart,
@@ -316,7 +316,6 @@
     res_copy.start()
 
     loads = [
-        pltpu.make_async_copy(tile, tiles.at[z], ld.at[0]),
         pltpu.make_async_copy(eg, gu.at[y, :, pl.ds(0, 128)], ld.at[1]),
         pltpu.make_async_copy(eu, gu.at[y, :, pl.ds(128, 128)], ld.at[2]),
         pltpu.make_async_copy(ed, dn.at[pl.ds(y * 128, 128)], ld.at[3]),
@@ -326,7 +325,15 @@
         pltpu.make_async_copy(wf, wfv, ld.at[7]),
         pltpu.make_async_copy(wh, whv, ld.at[8]),
     ]
-    loads[0].start()
+    table = jnp.concatenate([names_in[...].astype(F32), scale_in[...]], axis=0)
+    own_table = jnp.zeros((8, 128), F32)
+    for k in range(4):
+        own_table = own_table + pltpu.roll(table, (128 - 32 * k) % 128, 1) * (y == k).astype(F32)
+    own_table = jnp.where(lax.broadcasted_iota(jnp.int32, (8, 128), 1) < 32, own_table, 0.0)
+    spread = own_table
+    for k in (1, 2, 3):
+        spread = spread + pltpu.roll(own_table, 32 * k, 1)
+    tiles[z] = spread
 
     def hop(prt, idx, device):
         return pltpu.make_async_remote_copy(
@@ -357,7 +364,6 @@
         )
 
 
-    loads[0].wait()
     for k in range(1, 8):
         tile_copy(k).start()
 
@@ -378,7 +384,7 @@
     ups = up_rows(UP_ROWS, 4096 - UP_ROWS, 2)
     gates.start()
     ups0.start()
-    for copy in loads[1:]:
+    for copy in loads:
         copy.start()
 
     lane = lax.broadcasted_iota(jnp.int32, (128, 128), 1)
@@ -477,7 +483,7 @@
     att[:, 256:384] = jnp.where(lane < 64, outs[1][0], pltpu.roll(outs[1][1], 64, 1)).astype(BF)
     att[:, 384:512] = jnp.where(lane < 64, pltpu.roll(outs[2][0], 64, 1), outs[2][1]).astype(BF)
 
-    for copy in loads[7:]:
+    for copy in loads[6:]:
         copy.wait()
     asums = YReduce(part, far, near, rs_send, rs_recv, 1024)
     for n in range(4):
@@ -616,7 +622,7 @@
     fwd.relay(1)
     downs[2].relay()
     rows.start()
-    for copy in loads[1:7]:
+    for copy in loads[:6]:
         copy.wait()
     gates.finish()
     ups0.finish()
@@ -758,7 +764,8 @@
         layer_kernel,
         name="layer",
         out_shape=jax.ShapeDtypeStruct((32, D), BF),
-        in_specs=[vmem, anym, anym, vmem, vmem, anym, anym, vmem, anym, anym, anym, vmem] + [anym] * 7,
+        in_specs=[vmem, anym, anym, vmem, vmem, anym, anym, vmem, anym, anym, anym, vmem, vmem, vmem]
+        + [anym] * 6,
         out_specs=vmem,
         scratch_shapes=[
             bf(64, 128, 256), bf(64, 128, 256), bf(3, 256, 128),
@@ -788,12 +795,9 @@
     half_gates, residual, full_output, half_output, norm_gain, routes, route_weights,
     expert_gate, expert_up, expert_down, shared_gate, shared_up, shared_down,
 ):
-    quarter = lax.axis_index("tp")
-    own = lambda a: lax.dynamic_slice_in_dim(a.T.astype(F32), quarter * 32, 32, 1)
-    tile = jnp.tile(jnp.concatenate([own(routes), own(route_weights)], axis=0), (1, 4))
     return layer(
         full_queries, full_keys, full_values, full_gates.T, half_queries, half_keys, half_values,
-        half_gates.T, residual, full_output, half_output, norm_gain.reshape(1, D), tile,
+        half_gates.T, residual, full_output, half_output, norm_gain.reshape(1, D), routes.T, route_weights.T,
         expert_gate[0], expert_up[0], expert_down[0], shared_gate, shared_up, shared_down,
     )
 

time: 167 us -> 163 us (0.976)
  Pallas kernels: 163 us -> 160 us
    pallas_call x1, Pallas kernels: 163 us -> 160 us  [layer(): pl.pallas_call(layer_kernel, name='layer', out_shape=jax.ShapeDtypeStruct...]
where the time goes in v5:
time: 163 us; the launch traced here: 162 us
  Pallas kernels  160 us (98%)
  local copies, waits for them, and re-layouts  1.67 us (1%)
    pallas_call x1, Pallas kernels, layer(): pl.pallas_call(layer_kernel, name='layer', out_shape=jax.ShapeDtypeStruct...  160 us

profile of v5, /device:TPU:2, one launch (start us, length us, event | category | flops | bytes accessed | tf_op | source)
XLA Modules:
  0.0 161.7 jit_solution(16029183282665119363)
XLA Ops:
  0.0 160.0 %layer.1 = bf16[32,4096]{1,0:T(8,128)(2,1)} custom-call(bf16[128,256]{1,0:T(8,128)(2,1)} %fq.1, bf16[128,128]{1,0:T(8,128)(2,1)} %fk.1, bf16[128,128]{1,0:T(8,128)(2,1)} %fv.1, f32[2,8192]{1,0:T(2,128)} %bitcast.12, bf16[128,256]{1,0:T(8,128)(2,1)} %hq.1, bf16[128,128]{1,0:T(8,128)(2,1)} %hk.1, bf16[128,128]{1,0:T(8,128)(2,1)} %hv.1, f32[4,8192]{1,0:T(4,128)} %bitcast.11, ...), custom_call_target="tpu_custom_call" | custom-call | tf_op jit(solution)/shard_map/layer/pallas_call | solution.py:763
  160.0 1.7 %copy.22 = bf16[32,4096]{1,0:T(8,128)(2,1)} copy(bf16[32,4096]{1,0:T(8,128)(2,1)} %layer.1) | data formatting | bytes 524288

commit v6 on v5

--- a/solution.py
+++ b/solution.py
@@ -723,9 +723,9 @@
             downs[3].relay()
         if t == 2:
             rows.relay()
-        if t == 4:
+        if t == 5:
             shared()
-        if t == 6:
+        if t == 7:
             sums.relay(0)
         if t == 8:
             sums.arrived(0)

time: 163 us -> 162 us (level)
  no operation moved by 1% of the time
where the time goes in v6:
time: 162 us
  Pallas kernels  160 us (99%)
  local copies, waits for them, and re-layouts  1.67 us (1%)
    pallas_call x1, Pallas kernels, layer(): pl.pallas_call(layer_kernel, name='layer', out_shape=jax.ShapeDtypeStruct...  160 us

profile of v6, /device:TPU:2, one launch (start us, length us, event | category | flops | bytes accessed | tf_op | source)
XLA Modules:
  0.0 161.5 jit_solution(3816553046724494657)
XLA Ops:
  0.0 159.8 %layer.1 = bf16[32,4096]{1,0:T(8,128)(2,1)} custom-call(bf16[128,256]{1,0:T(8,128)(2,1)} %fq.1, bf16[128,128]{1,0:T(8,128)(2,1)} %fk.1, bf16[128,128]{1,0:T(8,128)(2,1)} %fv.1, f32[2,8192]{1,0:T(2,128)} %bitcast.12, bf16[128,256]{1,0:T(8,128)(2,1)} %hq.1, bf16[128,128]{1,0:T(8,128)(2,1)} %hk.1, bf16[128,128]{1,0:T(8,128)(2,1)} %hv.1, f32[4,8192]{1,0:T(4,128)} %bitcast.11, ...), custom_call_target="tpu_custom_call" | custom-call | tf_op jit(solution)/shard_map/layer/pallas_call | solution.py:763
  159.8 1.7 %copy.22 = bf16[32,4096]{1,0:T(8,128)(2,1)} copy(bf16[32,4096]{1,0:T(8,128)(2,1)} %layer.1) | data formatting | bytes 524288
